TPU v7x, 256 devices: a 4x2x16 block of a 4x16x16 slice. The times are simulated.
256 devices in a mesh: grp: 2 (over y), sp: 32 (over z, core), tp: 4 (over x).
Axes of the slice: x: 4, y: 2, z: 16, core: 2. Of those that a mesh axis runs over, the one named last changes fastest.
The devices are a block of a 4x16x16 slice.
Arguments:
- hidden_in: bfloat16 [16384, 2048], P(('grp', 'sp')), parts along dimension 0, may hold values from -6 to 6
- query_latent_rows: bfloat16 [16384, 768], P(('grp', 'sp')), parts along dimension 0, may hold values from -6 to 6
- key_value_latent: bfloat16 [16384, 512], P(('grp', 'sp')), parts along dimension 0, may hold values from -6 to 6
- rotary_key: bfloat16 [16384, 32], P(('grp', 'sp')), parts along dimension 0, may hold values from -64 to 64
- query_norm_gain: float32 [768], replicated, may hold values from 0.1 to 1.9
- key_value_gain: float32 [512], replicated, may hold values from 0.1 to 1.9
- query_up_weight: bfloat16 [768, 1536], P(None, 'tp'), may hold values from -0.625 to 0.625
- key_value_up_weight: bfloat16 [512, 2048], P(None, 'tp'), may hold values from -0.25 to 0.25
- out_proj: bfloat16 [1024, 2048], P('tp'), may hold values from -0.1875 to 0.1875
- feed_gain: float32 [2048], replicated, may hold values from 0.1 to 1.9
- feed_up: bfloat16 [2048, 8192], P('sp', 'tp'), may hold values from -0.125 to 0.125
- feed_down: bfloat16 [8192, 2048], P('tp', 'sp'), may hold values from -0.0625 to 0.0625
Outputs:
- layer_out: bfloat16 [16384, 2048], P(('grp', 'sp', 'tp')), parts along dimension 0
There are 2 independent parts, one for each index of `grp`. A program takes and returns all parts, laid end to end along the dimension named above; an argument that names none is the same for every part. Nothing has to cross between parts.
All inputs are finite; a program needn't handle non-finite values.
Results may differ from a plain program's by a relative error of at most 0.02.
Values may be sent and summed in bfloat16 or wider, within the bound.
A program may use at most 128 MiB of HBM per device.

v0:
```python
import math

import jax
import jax.numpy as jnp
from jax import lax
from jax.sharding import PartitionSpec as P

QUERY_KEY_PLAIN = 64
QUERY_KEY_ROTARY = 32
VALUE_HEAD_SIZE = 64


def cut_along(value, dim, count):
    before, after = (value.shape[:dim], value.shape[dim + 1 :])
    return jnp.moveaxis(value.reshape(*before, count, -1, *after), dim, 0)


def sum_at_owner(value, axis, dim):
    count = lax.axis_size(axis)
    pieces = lax.all_to_all(cut_along(value, dim, count), axis, 0, 0, tiled=True)
    return jnp.sum(pieces.astype(jnp.float32), axis=0)


def from_everyone(value, axis):
    copies = jnp.broadcast_to(value, (lax.axis_size(axis), *value.shape))
    return lax.all_to_all(copies, axis, split_axis=0, concat_axis=0, tiled=True)


def in_order(pieces, dim):
    lengths = list(pieces.shape[1:])
    lengths[dim] *= pieces.shape[0]
    return jnp.moveaxis(pieces, 0, dim).reshape(lengths)


def gather_directly(value, axis, dim):
    pieces = from_everyone(value, axis)
    return in_order(pieces, dim)


def normalize(values, gain):
    floats = values.astype(jnp.float32)
    return floats * lax.rsqrt(jnp.mean(floats * floats, axis=-1, keepdims=True) + 1e-06) * gain


def rotate(values, position):
    half_size = values.shape[-1] // 2
    inverse = 10000.0 ** (-jnp.arange(half_size, dtype=jnp.float32) * 2.0 / values.shape[-1])
    angles = position[:, None] * inverse[None, :]
    cosine = jnp.concatenate([jnp.cos(angles), jnp.cos(angles)], axis=-1)
    sine = jnp.concatenate([jnp.sin(angles), jnp.sin(angles)], axis=-1)
    shape = (values.shape[0],) + (1,) * (values.ndim - 2) + (values.shape[-1],)
    turned = jnp.concatenate([-values[..., half_size:], values[..., :half_size]], axis=-1)
    return values * cosine.reshape(shape) + turned * sine.reshape(shape)


def on_device(
    hidden_in,
    query_latent_rows,
    key_value_latent,
    rotary_key,
    query_norm_gain,
    key_value_gain,
    query_up_weight,
    key_value_up_weight,
    out_proj,
    feed_gain,
    feed_up,
    feed_down,
):
    tokens_here = hidden_in.shape[0]
    heads_here = query_up_weight.shape[1] // (QUERY_KEY_PLAIN + QUERY_KEY_ROTARY)
    position = (lax.axis_index("sp") * tokens_here + jnp.arange(tokens_here)).astype(jnp.float32)
    scale_factor = (QUERY_KEY_PLAIN + QUERY_KEY_ROTARY) ** (-0.5)
    query_norm = normalize(query_latent_rows, query_norm_gain).astype(jnp.bfloat16)
    queries = jnp.dot(query_norm, query_up_weight, preferred_element_type=jnp.float32).reshape(
        tokens_here, heads_here, QUERY_KEY_PLAIN + QUERY_KEY_ROTARY
    )
    queries = jnp.concatenate(
        [queries[..., :QUERY_KEY_PLAIN], rotate(queries[..., QUERY_KEY_PLAIN:], position)], axis=-1
    ).astype(jnp.bfloat16)
    query_plain = queries[..., :QUERY_KEY_PLAIN]
    query_turned = queries[..., QUERY_KEY_PLAIN:]
    latent = normalize(key_value_latent, key_value_gain).astype(jnp.bfloat16)
    key_rope = rotate(rotary_key.astype(jnp.float32), position).astype(jnp.bfloat16)

    def attend_block(carry, key_plain, value_rows, rope_rows):
        row_max, denom, accum = carry
        scores = jnp.einsum(
            "qhd,khd->hqk", query_plain, key_plain, preferred_element_type=jnp.float32
        )
        scores = scores + jnp.einsum(
            "qhd,kd->hqk", query_turned, rope_rows, preferred_element_type=jnp.float32
        )
        scores = scores * scale_factor
        new_max = jnp.maximum(row_max, jnp.max(scores, axis=-1))
        expo = jnp.exp(scores - new_max[:, :, None])
        factor = jnp.exp(row_max - new_max)
        denom = denom * factor + jnp.sum(expo, axis=-1)
        update = jnp.einsum(
            "hqk,khd->qhd",
            expo.astype(jnp.bfloat16),
            value_rows,
            preferred_element_type=jnp.float32,
        )
        accum = accum * jnp.transpose(factor)[:, :, None] + update
        return (new_max, denom, accum)

    start_carry = (
        jnp.full((heads_here, tokens_here), -1e30, jnp.float32),
        jnp.zeros((heads_here, tokens_here), jnp.float32),
        jnp.zeros((tokens_here, heads_here, VALUE_HEAD_SIZE), jnp.float32),
    )
    own_keys = jnp.dot(latent, key_value_up_weight, preferred_element_type=jnp.float32).astype(
        jnp.bfloat16
    )
    pieces = (
        lax.all_gather(own_keys, "sp", axis=0, tiled=True),
        lax.all_gather(key_rope, "sp", axis=0, tiled=True),
    )
    rows_in = pieces[0].shape[0]
    block = math.gcd(rows_in, 1024)

    def step_block(index, inner):
        first = index * block
        bulk = lax.dynamic_slice_in_dim(pieces[0], first, block, 0)
        rope_rows = lax.dynamic_slice_in_dim(pieces[1], first, block, 0)
        bulk = bulk.reshape(block, heads_here, QUERY_KEY_PLAIN + VALUE_HEAD_SIZE)
        return attend_block(
            inner, bulk[..., :QUERY_KEY_PLAIN], bulk[..., QUERY_KEY_PLAIN:], rope_rows
        )

    final_carry = lax.fori_loop(0, rows_in // block, step_block, start_carry)
    denom = final_carry[1]
    accum = final_carry[2]
    mixed = (
        (accum / jnp.transpose(denom)[:, :, None])
        .astype(jnp.bfloat16)
        .reshape(tokens_here, heads_here * VALUE_HEAD_SIZE)
    )
    share = tokens_here // lax.axis_size("tp")
    lead = lax.axis_index("tp") * share
    branch = sum_at_owner(
        jnp.dot(mixed, out_proj, preferred_element_type=jnp.float32).astype(jnp.bfloat16), "tp", 0
    )
    own_rows = lax.dynamic_slice_in_dim(hidden_in, lead, share, 0)
    middle_own = (own_rows.astype(jnp.float32) + branch).astype(jnp.bfloat16)
    normed = gather_directly(normalize(middle_own, feed_gain).astype(jnp.bfloat16), "tp", 0)
    upward = jnp.dot(
        normed,
        lax.all_gather(feed_up, "sp", axis=0, tiled=True),
        preferred_element_type=jnp.float32,
    )
    activated = jnp.square(jax.nn.relu(upward)).astype(jnp.bfloat16)
    partial_sum = jnp.dot(
        activated,
        lax.all_gather(feed_down, "sp", axis=1, tiled=True),
        preferred_element_type=jnp.float32,
    )
    feed = sum_at_owner(partial_sum.astype(jnp.bfloat16), "tp", 0)
    return (middle_own.astype(jnp.float32) + feed).astype(jnp.bfloat16)


def solution(mesh):
    return jax.shard_map(
        on_device,
        mesh=mesh,
        in_specs=(
            P(("grp", "sp"), None),
            P(("grp", "sp"), None),
            P(("grp", "sp"), None),
            P(("grp", "sp"), None),
            P(),
            P(),
            P(None, "tp"),
            P(None, "tp"),
            P("tp", None),
            P(),
            P("sp", "tp"),
            P("tp", "sp"),
        ),
        out_specs=P(("grp", "sp", "tp"), None),
        check_vma=False,
    )
```

profile of v0, /device:TPU:33, one launch (start us, length us, event | category | flops | bytes accessed | tf_op | source)
XLA Modules:
  0.0 289.8 jit_solution(13299205808065012109)
XLA Ops:
  7.7 2.2 convolution_convert_fusion.2
  14.2 1.6 fusion.32
  16.1 55.3 %all_gather.13 = bf16[8192,32]{0,1:T(8,128)(2,1)} all-gather(bf16[256,32]{0,1:T(8,128)(2,1)S(1)} %get-tuple-element.215), channel_id=1, replica_groups=mesh['grp'=2,'sp'=32,'tp'=4] {'sp'}, dimensions={0}, use_global_device_ids=true | all-gather | bytes 540672 | tf_op jit(solution)/shard_map/all_gather | solution.py:118
  72.0 30.9 %all-gather.4.cloned.1.call-done = bf16[8192,512]{1,0:T(8,128)(2,1)} async-done(((bf16[256,512]{1,0:T(8,128)(2,1)}), bf16[8192,512]{1,0:T(8,128)(2,1)}) %all-gather.4.cloned.1.call-update) | async-done | bytes 8388624 | tf_op jit(solution)/shard_map/all_gather | solution.py:117
  102.9 83.0 %while.18 = (s32[]{:T(128)}, f32[4,256]{1,0:T(4,128)S(1)}, f32[4,256]{1,0:T(4,128)S(1)}, f32[256,4,64]{0,2,1:T(8,128)S(1)}, bf16[8192,512]{1,0:T(8,128)(2,1)}, /...) while((s32[]{:T(128)}, f32[4,256]{1,0:T(4,128)S(1)}, ...), condition=%wide.region_5.0_spmd.clone, body=%wide.region_2.0_spmd.clone.sunk | while | flops 343087104 | bytes 44105964 | solution.py:132
  105.6 3.5 %fusion.71 = (f32[4,256]{1,0:T(4,128)S(1)}, f32[4,256,1024]{1,2,0:T(8,128)}) fusion(bf16[256,4,32]{0,2,1:T(8,128)(2,1)S(1)} %copy-done.2, bf16[8192,32]{0,1:T(8,128)(2,1)} %get-tuple-element.307, s32[]{:T(128)S(6)} %select_n.14, f32[4,1024,256]{2,1,0:T(8,128)S(1)} %fusion.70), kind=kOutput, calls=%fused_computation.74.clone.1 | convolution fusion | flops 70253568 | bytes 8523780 | tf_op jit(solution)/shard_map/while/body/eval_jaxpr/qhd,kd->hqk/dot_general | solution.py:91
  109.1 3.1 %fusion.75 = f32[256,4,64]{0,2,1:T(8,128)S(1)} fusion(f32[4,256,1024]{1,2,0:T(8,128)} %get-tuple-element.275, f32[4,256]{1,0:T(4,128)S(1)} %get-tuple-element.302, bf16[1024,4,128]{0,2,1:T(8,128)(2,1)S(1)} %bitcast.46, f32[256,4,64]{0,2,1:T(8,128)S(1)} %get-tuple-element.292, f32[256,4]{0,1:T(4,128)S(1)} %get-tuple-element.276, pred[]{:T(512)S(6)} %compare.3), kind=kOutput, calls=%fused_computation.8.clone.1 | convolution fusion | flops 136511488 | bytes 5251073 | tf_op jit(solution)/shard_map/while/body/eval_jaxpr/hqk,khd->qhd/dot_general | solution.py:99
  113.2 1.3 constant_dynamic-slice_fusion.2
  115.9 3.5 %fusion.71 = (f32[4,256]{1,0:T(4,128)S(1)}, f32[4,256,1024]{1,2,0:T(8,128)}) fusion(bf16[256,4,32]{0,2,1:T(8,128)(2,1)S(1)} %copy-done.2, bf16[8192,32]{0,1:T(8,128)(2,1)} %get-tuple-element.307, s32[]{:T(128)S(6)} %select_n.14, f32[4,1024,256]{2,1,0:T(8,128)S(1)} %fusion.70), kind=kOutput, calls=%fused_computation.74.clone.1 | convolution fusion | flops 70253568 | bytes 8523780 | tf_op jit(solution)/shard_map/while/body/eval_jaxpr/qhd,kd->hqk/dot_general | solution.py:91
  119.4 3.2 %fusion.75 = f32[256,4,64]{0,2,1:T(8,128)S(1)} fusion(f32[4,256,1024]{1,2,0:T(8,128)} %get-tuple-element.275, f32[4,256]{1,0:T(4,128)S(1)} %get-tuple-element.302, bf16[1024,4,128]{0,2,1:T(8,128)(2,1)S(1)} %bitcast.46, f32[256,4,64]{0,2,1:T(8,128)S(1)} %get-tuple-element.292, f32[256,4]{0,1:T(4,128)S(1)} %get-tuple-element.276, pred[]{:T(512)S(6)} %compare.3), kind=kOutput, calls=%fused_computation.8.clone.1 | convolution fusion | flops 136511488 | bytes 5251073 | tf_op jit(solution)/shard_map/while/body/eval_jaxpr/hqk,khd->qhd/dot_general | solution.py:99
  123.6 1.3 constant_dynamic-slice_fusion.2
  126.3 3.5 %fusion.71 = (f32[4,256]{1,0:T(4,128)S(1)}, f32[4,256,1024]{1,2,0:T(8,128)}) fusion(bf16[256,4,32]{0,2,1:T(8,128)(2,1)S(1)} %copy-done.2, bf16[8192,32]{0,1:T(8,128)(2,1)} %get-tuple-element.307, s32[]{:T(128)S(6)} %select_n.14, f32[4,1024,256]{2,1,0:T(8,128)S(1)} %fusion.70), kind=kOutput, calls=%fused_computation.74.clone.1 | convolution fusion | flops 70253568 | bytes 8523780 | tf_op jit(solution)/shard_map/while/body/eval_jaxpr/qhd,kd->hqk/dot_general | solution.py:91
  129.8 3.2 %fusion.75 = f32[256,4,64]{0,2,1:T(8,128)S(1)} fusion(f32[4,256,1024]{1,2,0:T(8,128)} %get-tuple-element.275, f32[4,256]{1,0:T(4,128)S(1)} %get-tuple-element.302, bf16[1024,4,128]{0,2,1:T(8,128)(2,1)S(1)} %bitcast.46, f32[256,4,64]{0,2,1:T(8,128)S(1)} %get-tuple-element.292, f32[256,4]{0,1:T(4,128)S(1)} %get-tuple-element.276, pred[]{:T(512)S(6)} %compare.3), kind=kOutput, calls=%fused_computation.8.clone.1 | convolution fusion | flops 136511488 | bytes 5251073 | tf_op jit(solution)/shard_map/while/body/eval_jaxpr/hqk,khd->qhd/dot_general | solution.py:99
  136.7 3.5 %fusion.71 = (f32[4,256]{1,0:T(4,128)S(1)}, f32[4,256,1024]{1,2,0:T(8,128)}) fusion(bf16[256,4,32]{0,2,1:T(8,128)(2,1)S(1)} %copy-done.2, bf16[8192,32]{0,1:T(8,128)(2,1)} %get-tuple-element.307, s32[]{:T(128)S(6)} %select_n.14, f32[4,1024,256]{2,1,0:T(8,128)S(1)} %fusion.70), kind=kOutput, calls=%fused_computation.74.clone.1 | convolution fusion | flops 70253568 | bytes 8523780 | tf_op jit(solution)/shard_map/while/body/eval_jaxpr/qhd,kd->hqk/dot_general | solution.py:91
  140.3 3.2 %fusion.75 = f32[256,4,64]{0,2,1:T(8,128)S(1)} fusion(f32[4,256,1024]{1,2,0:T(8,128)} %get-tuple-element.275, f32[4,256]{1,0:T(4,128)S(1)} %get-tuple-element.302, bf16[1024,4,128]{0,2,1:T(8,128)(2,1)S(1)} %bitcast.46, f32[256,4,64]{0,2,1:T(8,128)S(1)} %get-tuple-element.292, f32[256,4]{0,1:T(4,128)S(1)} %get-tuple-element.276, pred[]{:T(512)S(6)} %compare.3), kind=kOutput, calls=%fused_computation.8.clone.1 | convolution fusion | flops 136511488 | bytes 5251073 | tf_op jit(solution)/shard_map/while/body/eval_jaxpr/hqk,khd->qhd/dot_general | solution.py:99
  144.5 1.3 constant_dynamic-slice_fusion.2
  147.2 3.5 %fusion.71 = (f32[4,256]{1,0:T(4,128)S(1)}, f32[4,256,1024]{1,2,0:T(8,128)}) fusion(bf16[256,4,32]{0,2,1:T(8,128)(2,1)S(1)} %copy-done.2, bf16[8192,32]{0,1:T(8,128)(2,1)} %get-tuple-element.307, s32[]{:T(128)S(6)} %select_n.14, f32[4,1024,256]{2,1,0:T(8,128)S(1)} %fusion.70), kind=kOutput, calls=%fused_computation.74.clone.1 | convolution fusion | flops 70253568 | bytes 8523780 | tf_op jit(solution)/shard_map/while/body/eval_jaxpr/qhd,kd->hqk/dot_general | solution.py:91
  150.7 3.2 %fusion.75 = f32[256,4,64]{0,2,1:T(8,128)S(1)} fusion(f32[4,256,1024]{1,2,0:T(8,128)} %get-tuple-element.275, f32[4,256]{1,0:T(4,128)S(1)} %get-tuple-element.302, bf16[1024,4,128]{0,2,1:T(8,128)(2,1)S(1)} %bitcast.46, f32[256,4,64]{0,2,1:T(8,128)S(1)} %get-tuple-element.292, f32[256,4]{0,1:T(4,128)S(1)} %get-tuple-element.276, pred[]{:T(512)S(6)} %compare.3), kind=kOutput, calls=%fused_computation.8.clone.1 | convolution fusion | flops 136511488 | bytes 5251073 | tf_op jit(solution)/shard_map/while/body/eval_jaxpr/hqk,khd->qhd/dot_general | solution.py:99
  154.9 1.3 constant_dynamic-slice_fusion.2
  157.6 3.5 %fusion.71 = (f32[4,256]{1,0:T(4,128)S(1)}, f32[4,256,1024]{1,2,0:T(8,128)}) fusion(bf16[256,4,32]{0,2,1:T(8,128)(2,1)S(1)} %copy-done.2, bf16[8192,32]{0,1:T(8,128)(2,1)} %get-tuple-element.307, s32[]{:T(128)S(6)} %select_n.14, f32[4,1024,256]{2,1,0:T(8,128)S(1)} %fusion.70), kind=kOutput, calls=%fused_computation.74.clone.1 | convolution fusion | flops 70253568 | bytes 8523780 | tf_op jit(solution)/shard_map/while/body/eval_jaxpr/qhd,kd->hqk/dot_general | solution.py:91
  161.2 3.2 %fusion.75 = f32[256,4,64]{0,2,1:T(8,128)S(1)} fusion(f32[4,256,1024]{1,2,0:T(8,128)} %get-tuple-element.275, f32[4,256]{1,0:T(4,128)S(1)} %get-tuple-element.302, bf16[1024,4,128]{0,2,1:T(8,128)(2,1)S(1)} %bitcast.46, f32[256,4,64]{0,2,1:T(8,128)S(1)} %get-tuple-element.292, f32[256,4]{0,1:T(4,128)S(1)} %get-tuple-element.276, pred[]{:T(512)S(6)} %compare.3), kind=kOutput, calls=%fused_computation.8.clone.1 | convolution fusion | flops 136511488 | bytes 5251073 | tf_op jit(solution)/shard_map/while/body/eval_jaxpr/hqk,khd->qhd/dot_general | solution.py:99
  168.0 3.5 %fusion.71 = (f32[4,256]{1,0:T(4,128)S(1)}, f32[4,256,1024]{1,2,0:T(8,128)}) fusion(bf16[256,4,32]{0,2,1:T(8,128)(2,1)S(1)} %copy-done.2, bf16[8192,32]{0,1:T(8,128)(2,1)} %get-tuple-element.307, s32[]{:T(128)S(6)} %select_n.14, f32[4,1024,256]{2,1,0:T(8,128)S(1)} %fusion.70), kind=kOutput, calls=%fused_computation.74.clone.1 | convolution fusion | flops 70253568 | bytes 8523780 | tf_op jit(solution)/shard_map/while/body/eval_jaxpr/qhd,kd->hqk/dot_general | solution.py:91
  171.6 3.1 %fusion.75 = f32[256,4,64]{0,2,1:T(8,128)S(1)} fusion(f32[4,256,1024]{1,2,0:T(8,128)} %get-tuple-element.275, f32[4,256]{1,0:T(4,128)S(1)} %get-tuple-element.302, bf16[1024,4,128]{0,2,1:T(8,128)(2,1)S(1)} %bitcast.46, f32[256,4,64]{0,2,1:T(8,128)S(1)} %get-tuple-element.292, f32[256,4]{0,1:T(4,128)S(1)} %get-tuple-element.276, pred[]{:T(512)S(6)} %compare.3), kind=kOutput, calls=%fused_computation.8.clone.1 | convolution fusion | flops 136511488 | bytes 5251073 | tf_op jit(solution)/shard_map/while/body/eval_jaxpr/hqk,khd->qhd/dot_general | solution.py:99
  178.3 3.5 %fusion.71 = (f32[4,256]{1,0:T(4,128)S(1)}, f32[4,256,1024]{1,2,0:T(8,128)}) fusion(bf16[256,4,32]{0,2,1:T(8,128)(2,1)S(1)} %copy-done.2, bf16[8192,32]{0,1:T(8,128)(2,1)} %get-tuple-element.307, s32[]{:T(128)S(6)} %select_n.14, f32[4,1024,256]{2,1,0:T(8,128)S(1)} %fusion.70), kind=kOutput, calls=%fused_computation.74.clone.1 | convolution fusion | flops 70253568 | bytes 8523780 | tf_op jit(solution)/shard_map/while/body/eval_jaxpr/qhd,kd->hqk/dot_general | solution.py:91
  181.8 3.1 %fusion.75 = f32[256,4,64]{0,2,1:T(8,128)S(1)} fusion(f32[4,256,1024]{1,2,0:T(8,128)} %get-tuple-element.275, f32[4,256]{1,0:T(4,128)S(1)} %get-tuple-element.302, bf16[1024,4,128]{0,2,1:T(8,128)(2,1)S(1)} %bitcast.46, f32[256,4,64]{0,2,1:T(8,128)S(1)} %get-tuple-element.292, f32[256,4]{0,1:T(4,128)S(1)} %get-tuple-element.276, pred[]{:T(512)S(6)} %compare.3), kind=kOutput, calls=%fused_computation.8.clone.1 | convolution fusion | flops 136511488 | bytes 5251073 | tf_op jit(solution)/shard_map/while/body/eval_jaxpr/hqk,khd->qhd/dot_general | solution.py:99
  185.9 1.4 convolution_convert_fusion
  187.4 4.2 %all-to-all-start = ((bf16[4,64,2048]{2,1,0:T(8,128)(2,1)}), bf16[4,64,2048]{2,1,0:T(8,128)(2,1)S(1)}, u32[]{:S(2)}, u32[]{:S(2)}) async-start(bf16[4,64,2048]{2,1,0:T(8,128)(2,1)} %bitcast.3), calls=%async_computation | async-start | bytes 2097152 | tf_op jit(solution)/shard_map/all_to_all | solution.py:20
  191.5 14.8 %all-to-all-done = bf16[4,64,2048]{2,1,0:T(8,128)(2,1)S(1)} async-done(((bf16[4,64,2048]{2,1,0:T(8,128)(2,1)}), bf16[4,64,2048]{2,1,0:T(8,128)(2,1)S(1)}, u32[]{:S(2)}, u32[]{:S(2)}) %all-to-all-start) | async-done | bytes 1048608 | tf_op jit(solution)/shard_map/all_to_all | solution.py:20
  208.9 3.6 %all-to-all-start.1 = ((bf16[4,64,2048]{2,1,0:T(8,128)(2,1)}), bf16[4,64,2048]{2,1,0:T(8,128)(2,1)S(1)}, u32[]{:S(2)}, u32[]{:S(2)}) async-start(bf16[4,64,2048]{2,1,0:T(8,128)(2,1)} %broadcast_in_dim.17), calls=%async_computation.1 | async-start | bytes 2097152 | tf_op jit(solution)/shard_map/all_to_all | solution.py:26
  212.5 41.0 %all-gather.8.cloned.1.call-done = bf16[2048,2048]{0,1:T(8,128)(2,1)} async-done(((bf16[2048,64]{0,1:T(8,128)(2,1)}), bf16[2048,2048]{0,1:T(8,128)(2,1)}) %all-gather.8.cloned.1.call-update) | async-done | bytes 8388624 | tf_op jit(solution)/shard_map/all_gather | solution.py:156
  253.6 10.3 %convolution_convert_fusion.1 = bf16[256,2048]{1,0:T(8,128)(2,1)S(1)} fusion(bf16[2048,2048]{0,1:T(8,128)(2,1)} %all-gather.8.cloned.1.call-done, bf16[256,2048]{1,0:T(8,128)(2,1)S(1)} %bitcast.50, bf16[2048,2048]{1,0:T(8,128)(2,1)} %all-gather.6.cloned.1.call-done), kind=kOutput, calls=%fused_computation.26 | convolution fusion | flops 4297064448 | bytes 18874368 | tf_op jit(solution)/shard_map/dot_general | solution.py:154
  263.8 18.5 %all_to_all.15 = bf16[4,64,2048]{2,1,0:T(8,128)(2,1)S(1)} all-to-all(bf16[4,64,2048]{2,1,0:T(8,128)(2,1)S(1)} %bitcast.51), channel_id=1, replica_groups=mesh['grp'=2,'sp'=32,'tp'=4] {'tp'}, dimensions={0} | all-to-all | bytes 2097152 | tf_op jit(solution)/shard_map/all_to_all | solution.py:20
  (122 shorter events, 33.4 us)
Async XLA Ops:
  6.5 179.4 %copy-start = (bf16[256,2048]{1,0:T(8,128)(2,1)S(1)}, bf16[256,2048]{1,0:T(8,128)(2,1)}, u32[]{:S(2)}) copy-start(bf16[256,2048]{1,0:T(8,128)(2,1)} %param.22) | copy-start | bytes 3145732
  6.6 9.5 %copy-start.3 = (bf16[256,32]{0,1:T(8,128)(2,1)S(1)}, bf16[256,32]{0,1:T(8,128)(2,1)}, u32[]{:S(2)}) copy-start(bf16[256,32]{0,1:T(8,128)(2,1)} %param.17) | copy-start | bytes 49156
  6.6 96.4 %all-gather.4.cloned.1.call-start = ((), (), s32[]{:S(2)}) async-start(), calls=%async_computation.3 | async-start | bytes 8650752 | tf_op jit(solution)/shard_map/all_gather | solution.py:117
  10.0 202.5 %all-gather.6.cloned.1.call-start = ((), (), s32[]{:S(2)}) async-start(), calls=%async_computation.4 | async-start | bytes 8650752 | tf_op jit(solution)/shard_map/all_gather | solution.py:150
  10.8 242.7 %all-gather.8.cloned.1.call-start = ((), (), s32[]{:S(2)}) async-start(), calls=%async_computation.5 | async-start | bytes 8650752 | tf_op jit(solution)/shard_map/all_gather | solution.py:156
  104.8 0.8 copy-start.2
  109.1 3.4 %copy-start.1 = (f32[4,256,1024]{1,2,0:T(8,128)S(1)}, f32[4,256,1024]{1,2,0:T(8,128)}, u32[]{:S(2)}) copy-start(f32[4,256,1024]{1,2,0:T(8,128)} %get-tuple-element.275) | copy-start | bytes 12582916 | tf_op jit(solution)/shard_map/while
  115.0 0.8 copy-start.2
  119.4 3.6 %copy-start.1 = (f32[4,256,1024]{1,2,0:T(8,128)S(1)}, f32[4,256,1024]{1,2,0:T(8,128)}, u32[]{:S(2)}) copy-start(f32[4,256,1024]{1,2,0:T(8,128)} %get-tuple-element.275) | copy-start | bytes 12582916 | tf_op jit(solution)/shard_map/while
  125.5 0.8 copy-start.2
  129.8 3.6 %copy-start.1 = (f32[4,256,1024]{1,2,0:T(8,128)S(1)}, f32[4,256,1024]{1,2,0:T(8,128)}, u32[]{:S(2)}) copy-start(f32[4,256,1024]{1,2,0:T(8,128)} %get-tuple-element.275) | copy-start | bytes 12582916 | tf_op jit(solution)/shard_map/while
  135.9 0.8 copy-start.2
  140.3 3.6 %copy-start.1 = (f32[4,256,1024]{1,2,0:T(8,128)S(1)}, f32[4,256,1024]{1,2,0:T(8,128)}, u32[]{:S(2)}) copy-start(f32[4,256,1024]{1,2,0:T(8,128)} %get-tuple-element.275) | copy-start | bytes 12582916 | tf_op jit(solution)/shard_map/while
  146.3 0.8 copy-start.2
  150.7 3.6 %copy-start.1 = (f32[4,256,1024]{1,2,0:T(8,128)S(1)}, f32[4,256,1024]{1,2,0:T(8,128)}, u32[]{:S(2)}) copy-start(f32[4,256,1024]{1,2,0:T(8,128)} %get-tuple-element.275) | copy-start | bytes 12582916 | tf_op jit(solution)/shard_map/while
  156.8 0.8 copy-start.2
  161.2 3.6 %copy-start.1 = (f32[4,256,1024]{1,2,0:T(8,128)S(1)}, f32[4,256,1024]{1,2,0:T(8,128)}, u32[]{:S(2)}) copy-start(f32[4,256,1024]{1,2,0:T(8,128)} %get-tuple-element.275) | copy-start | bytes 12582916 | tf_op jit(solution)/shard_map/while
  167.2 0.8 copy-start.2
  171.6 3.4 %copy-start.1 = (f32[4,256,1024]{1,2,0:T(8,128)S(1)}, f32[4,256,1024]{1,2,0:T(8,128)}, u32[]{:S(2)}) copy-start(f32[4,256,1024]{1,2,0:T(8,128)} %get-tuple-element.275) | copy-start | bytes 12582916 | tf_op jit(solution)/shard_map/while
  177.5 0.8 copy-start.2
  181.8 3.4 %copy-start.1 = (f32[4,256,1024]{1,2,0:T(8,128)S(1)}, f32[4,256,1024]{1,2,0:T(8,128)}, u32[]{:S(2)}) copy-start(f32[4,256,1024]{1,2,0:T(8,128)} %get-tuple-element.275) | copy-start | bytes 12582916 | tf_op jit(solution)/shard_map/while
  185.9 21.7 %copy-start.4 = (f32[2048]{0:T(1024)S(1)}, f32[2048]{0:T(1024)}, u32[]{:S(2)}) copy-start(f32[2048]{0:T(1024)} %param.23) | copy-start | bytes 24580
  187.4 18.9 %all-to-all-start = ((bf16[4,64,2048]{2,1,0:T(8,128)(2,1)}), bf16[4,64,2048]{2,1,0:T(8,128)(2,1)S(1)}, u32[]{:S(2)}, u32[]{:S(2)}) async-start(bf16[4,64,2048]{2,1,0:T(8,128)(2,1)} %bitcast.3), calls=%async_computation | async-start | bytes 2097152 | tf_op jit(solution)/shard_map/all_to_all | solution.py:20
  208.9 44.7 %all-to-all-start.1 = ((bf16[4,64,2048]{2,1,0:T(8,128)(2,1)}), bf16[4,64,2048]{2,1,0:T(8,128)(2,1)S(1)}, u32[]{:S(2)}, u32[]{:S(2)}) async-start(bf16[4,64,2048]{2,1,0:T(8,128)(2,1)} %broadcast_in_dim.17), calls=%async_computation.1 | async-start | bytes 2097152 | tf_op jit(solution)/shard_map/all_to_all | solution.py:26
Sparse Core Ops, SparseCore 0:
  10.1 92.7 all-gather.3
  104.8 73.3 all-gather.5
  180.1 73.4 all-gather.7
where the time goes:
time: 291 us; the launch traced here: 290 us
  waiting for transfers between devices  88.2 us (30%)
  matrix products  75.2 us (26%)
  blocking collectives  73.7 us (25%)
  local copies, waits for them, and re-layouts  19.8 us (7%)
  between operations  13.3 us (5%)
  other arithmetic  11.1 us (4%)
  starting transfers between devices  7.9 us (3%)
    all_gather x1, blocking collectives, on_device(): lax.all_gather(key_rope, 'sp', axis=0, tiled=True)  55.3 us
    all_gather x1, waiting for transfers between devices, on_device(): lax.all_gather(feed_down, 'sp', axis=1, tiled=True)  41 us
    all_gather x1, waiting for transfers between devices, on_device(): lax.all_gather(own_keys, 'sp', axis=0, tiled=True)  30.9 us
    dot_general x8, matrix products, attend_block(): jnp.einsum('qhd,kd->hqk', query_turned, rope_rows, preferred_element_type...  28.1 us
    dot_general x8, matrix products, attend_block(): jnp.einsum('hqk,khd->qhd', expo.astype(jnp.bfloat16), value_rows, preferr...  25.4 us
    all_to_all x1, blocking collectives, sum_at_owner(): lax.all_to_all(cut_along(value, dim, count), axis, 0, 0, tiled=True)  18.5 us
    all_to_all x1, waiting for transfers between devices, sum_at_owner(): lax.all_to_all(cut_along(value, dim, count), axis, 0, 0, tiled=True)  14.8 us
    dynamic_slice x16, local copies, waits for them, and re-layouts, step_block(): bulk = lax.dynamic_slice_in_dim(pieces[0], first, block, 0)  14.7 us
  transfers between devices with their start and end apart: 5, of which 3 were waited for; matrix products, arithmetic and copies ran while one was open for 30% of the time, Pallas kernels for 0%

commit v1 on v0

v1 whole, which is shorter than its diff:
```python
import functools
import math

import jax
import jax.numpy as jnp
from jax import lax
from jax.experimental import pallas as pl
from jax.experimental.pallas import tpu as pltpu
from jax.sharding import PartitionSpec as P

PLAIN = 64
ROTARY = 32
VALUE = 64
MESH = pl.DeviceIdType.MESH
LANES = 128
SUB = 2


def normalize(values, gain):
    floats = values.astype(jnp.float32)
    return floats * lax.rsqrt(jnp.mean(floats * floats, axis=-1, keepdims=True) + 1e-06) * gain


def nt_dot(a, b):
    return lax.dot_general(a, b, (((1,), (1,)), ((), ())), preferred_element_type=jnp.float32)


def layer_kernel(
    Z, X,
    x_own, up_own, dn_own, hid, qp, qr, wk, wvt, wo, gain,
    out,
    xb, U, D, hrow, q2t, s_buf, vt, m_sc, l_sc, o_sc, mixed, bsend, brecv, mid, nb, act, osend, orecv,
    loc_s, lz_s, lz_r, lx1_s, lx1_r, lx2_s, lx2_r, ld_s, ld_r, wz_s, wz_r, wd_s, wd_r, wo_s, wo_r,
    rs_s, rs_r, ag_s, ag_r, fo_s, fo_r,
):
    HALF = Z // 2
    NT = SUB * HALF
    sp = lax.axis_index("sp")
    x = lax.axis_index("tp")
    z = sp // 2
    c = sp % 2
    sgn = 1 - 2 * c
    T = nb.shape[0]
    share = T // X
    shard = up_own.shape[0]
    srow = shard // SUB
    KB = wk.shape[0] // LANES
    qrows = x_own.shape[1]
    gsub = LANES // ROTARY
    grow = share // gsub
    keys = 4 * T
    gkeys = keys // gsub
    F = U.shape[1]
    W = U.shape[0]

    def at(zz):
        return lax.rem(zz + 2 * Z, Z)

    def zdev(zz):
        return {"sp": 2 * at(zz) + c}

    sib = {"sp": 2 * z + 1 - c}

    def xdev(d):
        return {"tp": lax.rem(x + d + X, X)}

    def rcopy(src, dst, ss, rs, dev):
        return pltpu.make_async_remote_copy(
            src_ref=src, dst_ref=dst, send_sem=ss, recv_sem=rs, device_id=dev, device_id_type=MESH
        )

    def zside(side, t):
        return at(z - t) if side == 0 else at(z + t)

    mine = x * share
    loads = [
        pltpu.make_async_copy(x_own, xb.at[z, c], loc_s.at[0]),
        pltpu.make_async_copy(up_own, U.at[pl.ds(pl.multiple_of(z * 2 * shard + c * shard, 32), shard)], loc_s.at[1]),
        pltpu.make_async_copy(dn_own, D.at[pl.ds(pl.multiple_of(z * 2 * shard + c * shard, 32), shard)], loc_s.at[2]),
        pltpu.make_async_copy(hid.at[pl.ds(pl.multiple_of(mine, share), share)], hrow, loc_s.at[3]),
    ]
    for load in loads:
        load.start()
    barrier = pltpu.get_barrier_semaphore()
    peers = [zdev(z + 1), zdev(z - 1), sib] + [xdev(d) for d in range(1, X)]
    for dev in peers:
        pl.semaphore_signal(barrier, inc=1, device_id=dev, device_id_type=MESH)
    pl.semaphore_wait(barrier, len(peers))
    for load in loads:
        load.wait()

    def lat(zz, core):
        return xb.at[zz, core, x]

    def lz_send(zz, side, hop, dev):
        rcopy(lat(zz, c), lat(zz, c), lz_s.at[side, hop], lz_r.at[side, hop], dev).start()

    def lz_wait(side, hop):
        rcopy(lat(z, c), lat(z, c), lz_s.at[side, hop], lz_r.at[side, hop], zdev(z + 1)).wait_recv()

    half_rows = qrows // 2
    def x1_send(zz, side, t):
        for i, d in enumerate((1, -1)):
            rcopy(xb.at[zz, c, x], xb.at[zz, c, x], lx1_s.at[i, side, t], lx1_r.at[i, side, t], xdev(d)).start()

    def x1_wait(side, t):
        for i, d in enumerate((1, -1)):
            rcopy(xb.at[z, c, x], xb.at[z, c, x], lx1_s.at[i, side, t], lx1_r.at[i, side, t], xdev(d)).wait_recv()

    def x2_part(zz, q, i):
        return xb.at[zz, c, q, pl.ds(i * 128, 128 if i == 0 else qrows - 128)]

    def x2_send(zz, side, t):
        for i, d in enumerate((1, -1)):
            part = x2_part(zz, lax.rem(x - d + X, X), i)
            rcopy(part, part, lx2_s.at[i, side, t], lx2_r.at[i, side, t], xdev(d)).start()

    def x2_wait(side, t):
        for i, d in enumerate((1, -1)):
            part = x2_part(z, x, i)
            rcopy(part, part, lx2_s.at[i, side, t], lx2_r.at[i, side, t], xdev(d)).wait_recv()

    def ld_send(zz, side, t):
        rcopy(xb.at[zz, c], xb.at[zz, c], ld_s.at[side, t], ld_r.at[side, t], sib).start()

    def ld_wait(side, t):
        rcopy(xb.at[z, c], xb.at[z, c], ld_s.at[side, t], ld_r.at[side, t], sib).wait_recv()

    weights = (U, D)

    def wslice(arr, zz, core, s):
        start = pl.multiple_of(zz * (2 * shard) + core * shard + s * srow, srow)
        return weights[arr].at[pl.ds(start, srow)]

    def wz_copy(arr, zz, side, k, dev):
        piece = wslice(arr, zz, c, lax.rem(k, SUB))
        return rcopy(piece, piece, wz_s.at[arr, side, k], wz_r.at[arr, side, k], dev)

    def wd_copy(arr, zz, side, k):
        piece = wslice(arr, zz, c, lax.rem(k, SUB))
        return rcopy(piece, piece, wd_s.at[arr, side, k], wd_r.at[arr, side, k], sib)

    def own_copy(arr):
        start = pl.multiple_of(z * 2 * shard + c * shard, shard)
        piece = weights[arr].at[pl.ds(start, shard)]
        return rcopy(piece, piece, wo_s.at[arr], wo_r.at[arr], sib)

    def w_first(arr):
        for k in range(SUB):
            if HALF > 1:
                wz_copy(arr, z, 0, jnp.int32(k), zdev(z + 1)).start()
                wz_copy(arr, z, 1, jnp.int32(k), zdev(z - 1)).start()
        own_copy(arr).start()

    def w_serve(arr, k):
        k = jnp.int32(k)
        hop = k // SUB + 1

        @pl.when(hop < HALF)
        def _():
            for side in range(2):
                wz_copy(arr, z, side, k, zdev(z + 1)).wait_recv()

        @pl.when(hop < HALF - 1)
        def _():
            wz_copy(arr, at(z - hop), 0, k + SUB, zdev(z + 1)).start()
            wz_copy(arr, at(z + hop), 1, k + SUB, zdev(z - 1)).start()

        @pl.when(hop == HALF - 1)
        def _():
            wz_copy(arr, at(z - hop * sgn), 0, k + SUB, zdev(z + sgn)).start()

        @pl.when(hop < HALF)
        def _():
            for side in range(2):
                wd_copy(arr, zside(side, hop), side, k).start()

        @pl.when(hop == HALF)
        def _():
            wz_copy(arr, z, 0, k, zdev(z + 1)).wait_recv()
            wd_copy(arr, at(z + HALF), 0, k).start()

    lz_send(z, 0, 1, zdev(z + 1))
    lz_send(z, 1, 1, zdev(z - 1))
    w_first(0)
    ld_send(z, 0, 0)

    tok = qp.shape[1]
    q2t[...] = jnp.zeros_like(q2t)
    for g in range(gsub):
        for p in range(2):
            for hh in range(2):
                h = 2 * p + hh
                q2t[g, p, hh * PLAIN:(hh + 1) * PLAIN, hh * tok:(hh + 1) * tok] = qp[h * PLAIN:(h + 1) * PLAIN, :]
                q2t[g, p, LANES + g * ROTARY:LANES + (g + 1) * ROTARY, hh * tok:(hh + 1) * tok] = (
                    qr[h * ROTARY:(h + 1) * ROTARY, :]
                )
    m_sc[...] = jnp.full_like(m_sc, -1e30)
    l_sc[...] = jnp.zeros_like(l_sc)
    o_sc[...] = jnp.zeros_like(o_sc)

    def attend(za, zb):
        for g in range(gsub):
            def rows(first, count):
                return jnp.concatenate(
                    [xb[zz, :, :, first:first + count, :].reshape(gkeys // 2, LANES) for zz in (za, zb)], axis=0
                )
            lhs = jnp.concatenate([rows(kb * share + g * grow, grow) for kb in range(KB)], axis=1)
            rope = rows(KB * share, grow)
            kk = jnp.dot(lhs, wk[...], preferred_element_type=jnp.float32).astype(jnp.bfloat16)
            vt[:, g * gkeys:(g + 1) * gkeys] = nt_dot(wvt[...], lhs).astype(jnp.bfloat16)
            for p in range(2):
                k2 = jnp.concatenate([kk[:, p * LANES:(p + 1) * LANES], rope], axis=1)
                s_buf[p, g * gkeys:(g + 1) * gkeys, :] = jnp.dot(
                    k2, q2t[g, p], preferred_element_type=jnp.float32
                )
        for p in range(2):
            old = m_sc[p:p + 1, :]
            new = jnp.maximum(old, jnp.max(s_buf[p], axis=0, keepdims=True))
            factor = jnp.exp2(old - new)
            m_sc[p:p + 1, :] = new
            expo = jnp.exp2(s_buf[p] - new)
            l_sc[p:p + 1, :] = l_sc[p:p + 1, :] * factor + jnp.sum(expo, axis=0, keepdims=True)
            weights_t = expo.astype(jnp.bfloat16)
            for hh in range(2):
                h = 2 * p + hh
                lanes = slice(hh * tok, (hh + 1) * tok)
                o_sc[h] = o_sc[h] * factor[:, lanes] + jnp.dot(
                    vt[h * VALUE:(h + 1) * VALUE, :], weights_t[:, lanes], preferred_element_type=jnp.float32
                )

    SKEW = 2

    def phase(i, carry):
        @pl.when(i < HALF)
        def _():
            for side in range(2):
                lz_wait(side, i)

        @pl.when(i < HALF - 1)
        def _():
            lz_send(at(z - i), 0, i + 1, zdev(z + 1))
            lz_send(at(z + i), 1, i + 1, zdev(z - 1))

        @pl.when(i == HALF - 1)
        def _():
            lz_send(at(z - i * sgn), 0, i + 1, zdev(z + sgn))

        @pl.when(i < HALF)
        def _():
            for side in range(2):
                x1_send(zside(side, i), side, i)

        @pl.when(i == HALF)
        def _():
            lz_wait(0, i)
            x1_send(at(z + HALF), 0, i)

        w_serve(0, i - 1)
        j = i - 1

        @pl.when((j >= 1) & (j < HALF))
        def _():
            for side in range(2):
                x1_wait(side, j)
            for side in range(2):
                x2_send(zside(side, j), side, j)

        @pl.when(j == HALF)
        def _():
            x1_wait(0, j)
            x2_send(at(z + HALF), 0, j)

        @pl.when(i > SKEW)
        def _():
            t = i - SKEW

            @pl.when(t < HALF)
            def _():
                for side in range(2):
                    ld_wait(side, t)

            @pl.when(t == HALF)
            def _():
                ld_wait(0, t)
                ld_wait(0, 0)

            attend(at(z - lax.rem(t, HALF)), at(z + t))

        @pl.when((j >= 1) & (j < HALF))
        def _():
            for side in range(2):
                x2_wait(side, j)
                ld_send(zside(side, j), side, j)

        @pl.when(j == HALF)
        def _():
            x2_wait(0, j)
            ld_send(at(z + HALF), 0, j)

        return carry

    lax.fori_loop(1, HALF + SKEW + 1, phase, 0)

    served = [HALF + SKEW]
    begun = [False]

    def serve_upto(n):
        while served[0] < min(n, 2 * NT):
            k = served[0]
            if k >= NT - 2 * SUB and not begun[0]:
                w_first(1)
                begun[0] = True
            w_serve(k // NT, k % NT)
            served[0] += 1

    heads = []
    for h in range(4):
        p, hh = h // 2, h % 2
        heads.append(o_sc[h] / l_sc[p:p + 1, hh * tok:(hh + 1) * tok])
    mixed[...] = jnp.transpose(jnp.concatenate(heads, axis=0)).astype(jnp.bfloat16)
    NB = 256
    def project(n, carry):
        cols = pl.ds(pl.multiple_of(n * NB, NB), NB)
        bsend[:, cols] = jnp.dot(mixed[...], wo[:, cols], preferred_element_type=jnp.float32).astype(jnp.bfloat16)
        return carry
    lax.fori_loop(0, W // NB, project, 0)

    def rowsof(q):
        return pl.ds(pl.multiple_of(q * share, share), share)

    branch = []
    for d in range(1, X):
        q = lax.rem(x + d, X)
        branch.append(rcopy(bsend.at[rowsof(q)], brecv.at[d - 1], rs_s.at[d - 1], rs_r.at[d - 1], xdev(d)))
        branch[-1].start()
    serve_upto(NT - 2)
    total = bsend[rowsof(x), :].astype(jnp.float32)
    for copy in branch:
        copy.wait_recv()
    for d in range(X - 1):
        total = total + brecv[d].astype(jnp.float32)
    middle = (hrow[...].astype(jnp.float32) + total).astype(jnp.bfloat16)
    mid[...] = middle
    nb[rowsof(x), :] = normalize(middle, gain[...]).astype(jnp.bfloat16)
    spread = []
    for d in range(1, X):
        spread.append(rcopy(nb.at[rowsof(x)], nb.at[rowsof(x)], ag_s.at[d - 1], ag_r.at[d - 1], xdev(d)))
        spread[-1].start()
    serve_upto(NT + 2)
    for copy in spread:
        copy.wait_recv()

    def wd_wait(arr, k):
        hop = k // SUB + 1
        for side in range(2 if hop < HALF else 1):
            wd_copy(arr, z, side, jnp.int32(k)).wait_recv()

    own_copy(0).wait_recv()
    for k in range(NT):
        wd_wait(0, k)
    CUTS = 4
    per = F // NB // CUTS
    for cut in range(CUTS):
        def up(n, carry):
            cols = pl.ds(pl.multiple_of(n * NB, NB), NB)
            high = jnp.maximum(jnp.dot(nb[...], U[:, cols], preferred_element_type=jnp.float32), 0.0)
            act[:, cols] = (high * high).astype(jnp.bfloat16)
            return carry
        lax.fori_loop(cut * per, (cut + 1) * per, up, 0)
        if cut < CUTS - 1:
            serve_upto(NT + 3 + cut)

    def fo_copy(t, d):
        q = lax.rem(x + d, X)
        return rcopy(osend.at[t, q], orecv.at[t, d - 1], fo_s.at[t, d - 1], fo_r.at[t, d - 1], xdev(d))

    def pair_of(t):
        return at(z - (t % HALF)), at(z + t)

    for t in range(1, HALF + 1):
        serve_upto(NT + 2 * t)
        if t == HALF:
            own_copy(1).wait_recv()
        for k in (2 * t - 2, 2 * t - 1):
            wd_wait(1, k)
        rhs = jnp.concatenate(
            [D[pl.ds(pl.multiple_of(zz * 2 * shard, 2 * shard), 2 * shard), :] for zz in pair_of(t)], axis=0
        )
        block = nt_dot(act[...], rhs).astype(jnp.bfloat16)
        for q in range(X):
            for side in range(2):
                osend[t - 1, q, side] = block[q * share:(q + 1) * share, side * LANES:(side + 1) * LANES]
        for d in range(1, X):
            fo_copy(t - 1, d).start()
    for t in range(1, HALF + 1):
        for d in range(1, X):
            fo_copy(t - 1, d).wait_recv()
        for side, zz in enumerate(pair_of(t)):
            cols = pl.ds(pl.multiple_of(zz * LANES, LANES), LANES)
            total = osend[t - 1, x, side].astype(jnp.float32)
            for d in range(X - 1):
                total = total + orecv[t - 1, d, side].astype(jnp.float32)
            out[:, cols] = (mid[:, cols].astype(jnp.float32) + total).astype(jnp.bfloat16)

    for copy in branch + spread:
        copy.wait_send()
    for t in range(HALF):
        for d in range(1, X):
            fo_copy(t, d).wait_send()
    ld_wait_s = lambda side, t: rcopy(xb.at[z, c], xb.at[z, c], ld_s.at[side, t], ld_r.at[side, t], sib).wait_send()
    ld_wait_s(0, 0)
    for arr in range(2):
        own_copy(arr).wait_send()

    def drain(t, carry):
        def both(side):
            rcopy(lat(z, c), lat(z, c), lz_s.at[side, t], lz_r.at[side, t], zdev(z + 1)).wait_send()
            for i, d in enumerate((1, -1)):
                rcopy(xb.at[z, c, x], xb.at[z, c, x], lx1_s.at[i, side, t], lx1_r.at[i, side, t], xdev(d)).wait_send()
                part = x2_part(z, x, i)
                rcopy(part, part, lx2_s.at[i, side, t], lx2_r.at[i, side, t], xdev(d)).wait_send()
            ld_wait_s(side, t)
            for arr in range(2):
                for s in range(SUB):
                    k = (t - 1) * SUB + s
                    wz_copy(arr, z, side, k, zdev(z + 1)).wait_send()
                    wd_copy(arr, z, side, k).wait_send()
        both(0)
        pl.when(t < HALF)(lambda: both(1))
        return carry
    lax.fori_loop(1, HALF + 1, drain, 0)


def fused_layer(Z, X, x_own, up_own, dn_own, hid, qp, qr, wk, wvt, wo, gain, F):
    HALF = Z // 2
    NT = SUB * HALF
    T, W = hid.shape
    share = T // X
    bf, f32 = jnp.bfloat16, jnp.float32
    DMA = pltpu.SemaphoreType.DMA
    any_ = pl.BlockSpec(memory_space=pl.ANY)
    vm = pl.BlockSpec(memory_space=pltpu.VMEM)
    scratch = [
        pltpu.VMEM((Z, 2) + x_own.shape, bf),
        pltpu.VMEM((W, F), bf),
        pltpu.VMEM((W, F), bf),
        pltpu.VMEM((share, W), bf),
        pltpu.VMEM((LANES // ROTARY, 2, 2 * LANES, 2 * T), bf),
        pltpu.VMEM((2, 4 * T, 2 * T), f32),
        pltpu.VMEM((wvt.shape[0], 4 * T), bf),
        pltpu.VMEM((2, 2 * T), f32),
        pltpu.VMEM((2, 2 * T), f32),
        pltpu.VMEM((4, VALUE, T), f32),
        pltpu.VMEM((T, 4 * VALUE), bf),
        pltpu.VMEM((T, W), bf),
        pltpu.VMEM((X - 1, share, W), bf),
        pltpu.VMEM((share, W), bf),
        pltpu.VMEM((T, W), bf),
        pltpu.VMEM((T, F), bf),
        pltpu.VMEM((HALF, X, 2, share, LANES), bf),
        pltpu.VMEM((HALF, X - 1, 2, share, LANES), bf),
        DMA((4,)),
        DMA((2, HALF + 1)), DMA((2, HALF + 1)),
        DMA((2, 2, HALF + 1)), DMA((2, 2, HALF + 1)),
        DMA((2, 2, HALF + 1)), DMA((2, 2, HALF + 1)),
        DMA((2, HALF + 1)), DMA((2, HALF + 1)),
        DMA((2, 2, NT)), DMA((2, 2, NT)),
        DMA((2, 2, NT)), DMA((2, 2, NT)),
        DMA((2,)), DMA((2,)),
        DMA((X - 1,)), DMA((X - 1,)),
        DMA((X - 1,)), DMA((X - 1,)),
        DMA((HALF, X - 1)), DMA((HALF, X - 1)),
    ]
    return pl.pallas_call(
        functools.partial(layer_kernel, Z, X),
        out_shape=jax.ShapeDtypeStruct((share, W), bf),
        in_specs=[any_, any_, any_, any_, vm, vm, vm, vm, vm, vm],
        out_specs=vm,
        scratch_shapes=scratch,
        compiler_params=pltpu.CompilerParams(
            collective_id=0, has_side_effects=True, vmem_limit_bytes=62 * 1024 * 1024
        ),
        name="layer",
    )(x_own, up_own, dn_own, hid, qp, qr, wk, wvt, wo, gain)


def on_device(
    hidden_in, query_latent_rows, key_value_latent, rotary_key, query_norm_gain, key_value_gain,
    query_up_weight, key_value_up_weight, out_proj, feed_gain, feed_up, feed_down,
):
    X = lax.axis_size("tp")
    Z = lax.axis_size("sp") // 2
    T = hidden_in.shape[0]
    heads = query_up_weight.shape[1] // (PLAIN + ROTARY)
    share = T // X
    half = ROTARY // 2
    position = (lax.axis_index("sp") * T + jnp.arange(T)).astype(jnp.float32)
    inverse = 10000.0 ** (-jnp.arange(half, dtype=jnp.float32) * 2.0 / ROTARY)
    angles = position[:, None] * inverse[None, :]
    cosine, sine = jnp.cos(angles), jnp.sin(angles)
    scale = (PLAIN + ROTARY) ** (-0.5) * math.log2(math.e)

    query_norm = normalize(query_latent_rows, query_norm_gain).astype(jnp.bfloat16)
    queries = jnp.dot(query_norm, query_up_weight, preferred_element_type=jnp.float32)
    queries = queries.reshape(T, heads, PLAIN + ROTARY) * scale
    first, second = queries[..., PLAIN:PLAIN + half], queries[..., PLAIN + half:]
    cq, sq = cosine[:, None, :], sine[:, None, :]
    turned = jnp.concatenate([first * cq - second * sq, second * cq + first * sq], axis=-1)
    qp = queries[..., :PLAIN].astype(jnp.bfloat16).reshape(T, heads * PLAIN).T
    qr = turned.astype(jnp.bfloat16).reshape(T, heads * ROTARY).T

    latent = normalize(key_value_latent, key_value_gain).astype(jnp.bfloat16)
    key = rotary_key.astype(jnp.float32)
    k1, k2 = key[:, :half], key[:, half:]
    key_rope = jnp.concatenate([k1 * cosine - k2 * sine, k2 * cosine + k1 * sine], axis=-1).astype(jnp.bfloat16)
    KB = latent.shape[1] // LANES
    groups = LANES // ROTARY
    packed = latent.reshape(X, share, KB, LANES).transpose(0, 2, 1, 3).reshape(X, KB * share, LANES)
    ropes = key_rope.reshape(X, groups, share // groups, ROTARY).transpose(0, 2, 1, 3)
    x_own = jnp.concatenate([packed, ropes.reshape(X, share // groups, LANES)], axis=1)

    both = key_value_up_weight.reshape(-1, heads, PLAIN + VALUE)
    wk = both[..., :PLAIN].reshape(-1, heads * PLAIN)
    wvt = both[..., PLAIN:].reshape(-1, heads * VALUE).T
    return fused_layer(
        Z, X, x_own, feed_up, feed_down.T, hidden_in, qp, qr, wk, wvt, out_proj,
        feed_gain.reshape(1, -1), feed_up.shape[1],
    )


def solution(mesh):
    return jax.shard_map(
        on_device,
        mesh=mesh,
        in_specs=(
            P(("grp", "sp"), None),
            P(("grp", "sp"), None),
            P(("grp", "sp"), None),
            P(("grp", "sp"), None),
            P(),
            P(),
            P(None, "tp"),
            P(None, "tp"),
            P("tp", None),
            P(),
            P("sp", "tp"),
            P("tp", "sp"),
        ),
        out_specs=P(("grp", "sp", "tp"), None),
        check_vma=False,
    )
```

time: 291 us -> 172 us (0.59)
  Pallas kernels: 0 us -> 162 us
  waiting for transfers between devices: 88.2 us -> 0 us
  matrix products: 75.2 us -> 0.43 us
  blocking collectives: 73.7 us -> 0 us
  local copies, waits for them, and re-layouts: 19.8 us -> 6.52 us
  between operations: 13.3 us -> 0.15 us
  other arithmetic: 11.1 us -> 3.15 us
  starting transfers between devices: 7.9 us -> 0 us
    pallas_call x0 -> x1, Pallas kernels: none -> 162 us  [fused_layer(): pl.pallas_call(functools.partial(layer_kernel, Z, X), out_shape=jax.Shape...]
    dot_general x27 -> x0, matrix products: 73.6 us -> none  [the longest x8 28.1 us: attend_block(): jnp.einsum('qhd,kd->hqk', query_turned, rope_rows, preferred_element_type...]
    all_gather x3 -> x0, waiting for transfers between devices: 71.9 us -> none  [the longest x1 41 us: on_device(): lax.all_gather(feed_down, 'sp', axis=1, tiled=True)]
    all_gather x1 -> x0, blocking collectives: 55.3 us -> none  [on_device(): lax.all_gather(key_rope, 'sp', axis=0, tiled=True)]
    all_to_all x1 -> x0, blocking collectives: 18.5 us -> none  [sum_at_owner(): lax.all_to_all(cut_along(value, dim, count), axis, 0, 0, tiled=True)]
    all_to_all x2 -> x0, waiting for transfers between devices: 14.8 us -> none  [the longest x1 14.8 us: sum_at_owner(): lax.all_to_all(cut_along(value, dim, count), axis, 0, 0, tiled=True)]
    dynamic_slice x16 -> x0, local copies, waits for them, and re-layouts: 14.7 us -> none  [step_block(): bulk = lax.dynamic_slice_in_dim(pieces[0], first, block, 0)]
    all_to_all x2 -> x0, starting transfers between devices: 7.77 us -> none  [the longest x1 4.16 us: sum_at_owner(): lax.all_to_all(cut_along(value, dim, count), axis, 0, 0, tiled=True)]
  transfers between devices with their start and end apart: 5 -> 0, of which waited for: 3 -> 0; matrix products, arithmetic and copies ran while one was open for 30% -> 0% of each run, Pallas kernels for 0% -> 0%
where the time goes in v1:
time: 172 us
  Pallas kernels  162 us (94%)
  local copies, waits for them, and re-layouts  6.52 us (4%)
  other arithmetic  3.15 us (2%)
    pallas_call x1, Pallas kernels, fused_layer(): pl.pallas_call(functools.partial(layer_kernel, Z, X), out_shape=jax.Shape...  162 us

profile of v1, /device:TPU:33, one launch (start us, length us, event | category | flops | bytes accessed | tf_op | source)
XLA Modules:
  0.0 171.9 jit_solution(8364983812766227676)
XLA Ops:
  0.0 1.2 fusion
  1.3 0.0 copy-done.1
  1.3 0.0 copy-start.4
  1.3 0.1 fusion.3
  1.4 0.6 copy-done.4
  2.0 0.1 multiply_cosine_fusion
  2.2 0.1 concatenate.17
  2.3 0.1 copy.22
  2.4 0.1 concatenate.16
  2.5 0.1 copy.21
  2.7 0.1 maximum_bitcast_fusion
  2.8 0.0 copy-start.5
  2.8 0.1 reshape.113
  2.9 0.6 copy-done.5
  3.5 0.1 fusion.5
  3.6 0.1 reshape.111
  3.7 0.0 copy-start.3
  3.7 0.0 copy-start.6
  3.7 0.7 pad_maximum_fusion.x_own
  4.5 0.0 copy-done
  4.5 0.3 copy-done.3
  4.8 0.0 copy-done.6
  4.8 0.4 convolution_multiply_fusion
  5.3 0.0 copy-start.2
  5.3 0.2 copy.23
  5.5 0.7 slice.45
  6.1 0.6 pad_maximum_fusion.1
  6.8 0.2 copy.24
  7.0 0.8 fusion.9
  7.7 0.8 copy.25.wk
  8.6 161.7 %layer.1 = bf16[64,2048]{1,0:T(8,128)(2,1)} custom-call(bf16[4,272,128]{2,1,0:T(8,128)(2,1)} %pad_maximum_fusion.x_own, bf16[64,2048]{1,0:T(8,128)(2,1)} %up_own.1, bf16[64,2048]{1,0:T(8,128)(2,1)} %bitcast.32, bf16[256,2048]{1,0:T(8,128)(2,1)} %hid.1, bf16[256,256]{1,0:T(8,128)(2,1)} %bitcast.30, bf16[128,256]{1,0:T(8,128)(2,1)} %bitcast.31, ...), custom_call_target="tpu_custom_call" | custom-call | tf_op jit(solution)/shard_map/layer/pallas_call | solution.py:475
  170.3 1.7 copy.27
  (10 shorter events, 0.1 us)
Async XLA Ops:
  0.0 4.5 %copy-start = (bf16[768,384]{1,0:T(8,128)(2,1)S(1)}, bf16[768,384]{1,0:T(8,128)(2,1)}, u32[]{:S(2)}) copy-start(bf16[768,384]{1,0:T(8,128)(2,1)} %param.18) | copy-start | bytes 1769476
  0.0 1.3 copy-start.1
  1.3 0.7 copy-start.4
  2.8 0.7 copy-start.5
  3.7 1.1 copy-start.3
  3.7 1.1 copy-start.6
  5.3 1.5 copy-start.2

commit v2 on v1

v2 whole, which is shorter than its diff:
```python
import functools
import math

import jax
import jax.numpy as jnp
from jax import lax
from jax.experimental import pallas as pl
from jax.experimental.pallas import tpu as pltpu
from jax.sharding import PartitionSpec as P

PLAIN = 64
ROTARY = 32
VALUE = 64
MESH = pl.DeviceIdType.MESH
LANES = 128


def normalize(values, gain_ref):
    floats = values.astype(jnp.float32)
    inverse = lax.rsqrt(jnp.mean(floats * floats, axis=-1, keepdims=True) + 1e-06)
    return jnp.concatenate(
        [
            floats[:, k * LANES:(k + 1) * LANES] * inverse * gain_ref[k:k + 1, :]
            for k in range(values.shape[1] // LANES)
        ],
        axis=1,
    ).astype(jnp.bfloat16)


def nt_dot(a, b):
    return lax.dot_general(a, b, (((1,), (1,)), ((), ())), preferred_element_type=jnp.float32)


def layer_kernel(
    Z, X, paired,
    kvl, key_t, up_own, dn_own, hid, ql, wq, wkv, wo, cos_t, sin_t, q_gain, kv_gain, gain,
    out,
    xb, turned_key, U, D, hrow, WKV, WO, qx, q2t, wk, wvt, s_buf, m_sc, l_sc, o_sc, obuf, orx, relay, lse, wts, msend, mixed,
    mid, nb, act, osend, orecv, opart, ofar,
    loc_s, lz_s, lz_r, ld_s, ld_r, wz_s, wz_r, wy_s, wy_r, wd_s, wd_r, yd_s, yd_r, wo_s, wo_r,
    x1_s, x1_r, x2_s, x2_r, xd_s, xd_r, ml_s, ml_r, mo_s, mo_r, mh_s, mh_r, mr_s, mr_r, md_s, md_r,
    ag_s, ag_r, ah_s, ah_r, fa_s, fa_r, fo_s, fo_r, fz_s, fz_r,
):
    HALF = Z // 2
    sp = lax.axis_index("sp")
    x = lax.axis_index("tp")
    z = sp // 2
    c = sp % 2
    sgn = 1 - 2 * c
    group = lax.axis_index("grp")
    par = group % 2
    T, W = nb.shape
    F = U.shape[1]
    share = T // X
    shard = up_own.shape[0]
    KB = kvl.shape[1] // LANES
    gsub = LANES // ROTARY
    grow = share // gsub
    HP = wkv.shape[1] // (PLAIN + VALUE)
    HC = HP * X // 2
    bf = jnp.bfloat16
    f32 = jnp.float32

    def at(zz):
        return lax.rem(zz + 2 * Z, Z)

    def zdev(zz):
        return {"sp": 2 * at(zz) + c}

    sib = {"sp": 2 * z + 1 - c}
    twin = {"grp": group + 1 - 2 * par}

    def xat(d):
        return lax.rem(x + d + X, X)

    def xdev(d):
        return {"tp": xat(d)}

    def rcopy(src, dst, ss, rs, dev):
        return pltpu.make_async_remote_copy(
            src_ref=src, dst_ref=dst, send_sem=ss, recv_sem=rs, device_id=dev, device_id_type=MESH
        )

    def zside(side, t):
        return at(z - t) if side == 0 else at(z + t)

    def shard_at(zz, core):
        return pl.multiple_of(zz * (2 * shard) + core * shard, shard)

    def rowsof(q):
        return pl.ds(pl.multiple_of(q * share, share), share)

    loads = [
        pltpu.make_async_copy(wkv, WKV.at[x], loc_s.at[0]),
        pltpu.make_async_copy(up_own, U.at[pl.ds(shard_at(z, c), shard)], loc_s.at[1]),
        pltpu.make_async_copy(wo, WO.at[x], loc_s.at[2]),
        pltpu.make_async_copy(hid.at[rowsof(x)], hrow, loc_s.at[3]),
        pltpu.make_async_copy(dn_own, D.at[pl.ds(shard_at(z, c), shard)], loc_s.at[4]),
    ]
    for load in loads:
        load.start()
    barrier = pltpu.get_barrier_semaphore()
    peers = [zdev(z + 1), zdev(z - 1), sib] + [xdev(d) for d in range(1, X)] + ([twin] if paired else [])
    for dev in peers:
        pl.semaphore_signal(barrier, inc=1, device_id=dev, device_id_type=MESH)

    latent = normalize(kvl[rowsof(x), :], kv_gain)
    for kb in range(KB):
        xb[z, c, kb * share:(kb + 1) * share, :] = latent[:, kb * LANES:(kb + 1) * LANES]
    cosine, sine = cos_t[...], sin_t[...]
    half = ROTARY // 2
    key_first = key_t[0:half, :].astype(f32)
    key_second = key_t[half:ROTARY, :].astype(f32)
    turned_key[...] = jnp.transpose(
        jnp.concatenate(
            [
                key_first * cosine - key_second * sine,
                key_second * cosine + key_first * sine,
                jnp.zeros((LANES - ROTARY, T), f32),
            ],
            axis=0,
        )
    )
    packed_key = 0.0
    for g in range(gsub):
        piece = turned_key[pl.ds(pl.multiple_of(x * share + g * grow, grow), grow), :]
        packed_key = packed_key + (piece if g == 0 else pltpu.roll(piece, g * ROTARY, 1))
    xb[z, c, KB * share:, :] = packed_key.astype(bf)
    pl.semaphore_wait(barrier, len(peers))

    def lz_copy(zz, side, hop, dev):
        piece = xb.at[zz, c]
        return rcopy(piece, piece, lz_s.at[side, hop], lz_r.at[side, hop], dev)

    def ld_copy(zz, side, t):
        return rcopy(xb.at[zz, c], xb.at[zz, c], ld_s.at[side, t], ld_r.at[side, t], sib)

    def lz_step(i):
        i = jnp.int32(i)

        @pl.when(i < HALF)
        def _():
            for side in range(2):
                lz_copy(z, side, i, zdev(z + 1)).wait_recv()

        @pl.when(i < HALF - 1)
        def _():
            lz_copy(at(z - i), 0, i + 1, zdev(z + 1)).start()
            lz_copy(at(z + i), 1, i + 1, zdev(z - 1)).start()

        @pl.when(i == HALF - 1)
        def _():
            lz_copy(at(z - i * sgn), 0, i + 1, zdev(z + sgn)).start()

        @pl.when(i < HALF)
        def _():
            for side in range(2):
                ld_copy(zside(side, i), side, i).start()

        @pl.when(i == HALF)
        def _():
            lz_copy(z, 0, i, zdev(z + 1)).wait_recv()
            ld_copy(at(z + HALF), 0, i).start()

    kv_half, q_half, o_half = WKV.shape[1] // 2, qx.shape[2], WO.shape[1] // 2

    def x_piece(what, q, lo=0, parts=1):
        if what == 0:
            n = kv_half // parts
            return WKV.at[q, pl.ds(pl.multiple_of(c * kv_half + lo * n, n), n)]
        if what == 1:
            n = q_half // parts
            return qx.at[q, c, pl.ds(lo * n, n)]
        n = o_half // parts
        return WO.at[q, pl.ds(pl.multiple_of(c * o_half + lo * n, n), n)]

    def x1_copy(what, i, d):
        piece = x_piece(what, x)
        return rcopy(piece, piece, x1_s.at[what, i], x1_r.at[what, i], xdev(d))

    def x2_copy(what, i, d):
        piece = x_piece(what, xat(-d), i, 2)
        return rcopy(piece, piece, x2_s.at[what, i], x2_r.at[what, i], xdev(d))

    def xd_copy(what, n):
        if what == 2:
            piece = x_piece(2, xat(n + 1))
        else:
            piece = x_piece(what, (1 - c) * (X // 2) + n)
        return rcopy(piece, piece, xd_s.at[what, n], xd_r.at[what, n], sib)

    def x_first(what):
        for i, d in enumerate((1, -1)):
            x1_copy(what, i, d).start()

    def x_relay(what):
        for i, d in enumerate((1, -1)):
            x1_copy(what, i, d).wait_recv()
            x2_copy(what, i, d).start()

    def x_share(what):
        for i, d in enumerate((1, -1)):
            x2_copy(what, i, d).wait_recv()
        for n in range(X - 1 if what == 2 else X // 2):
            if what == 0:
                pl.when((1 - c) * (X // 2) + n != x)(lambda: xd_copy(0, n).start())
            else:
                xd_copy(what, n).start()

    def x_end(what):
        for n in range(X - 1 if what == 2 else X // 2):
            if what == 0:
                pl.when(c * (X // 2) + n != x)(lambda: xd_copy(0, n).wait_recv())
            else:
                xd_copy(what, n).wait_recv()

    weights = (U, D)
    ZW = 3 if paired else 4
    part = shard // 4
    NP = ZW * HALF

    def place(zz, turn):
        return pl.ds(pl.multiple_of(shard_at(zz, c) + part * turn, part), part)

    def z_piece(arr, zz, k):
        s = lax.rem(k, ZW)
        return weights[arr].at[place(zz, jnp.where(s == 2, 2 + par, s) if paired else s)]

    def y_piece(arr, zz, turn):
        return weights[arr].at[place(zz, 2 + turn)]

    def wz_copy(arr, zz, side, k, dev):
        piece = z_piece(arr, zz, k)
        return rcopy(piece, piece, wz_s.at[arr, side, k], wz_r.at[arr, side, k], dev)

    def wy_copy(arr, zz, side, hop, turn):
        piece = y_piece(arr, zz, turn)
        return rcopy(piece, piece, wy_s.at[arr, side, hop], wy_r.at[arr, side, hop], twin)

    def wd_copy(arr, zz, side, k):
        piece = z_piece(arr, zz, k)
        return rcopy(piece, piece, wd_s.at[arr, side, k], wd_r.at[arr, side, k], sib)

    def yd_copy(arr, zz, side, hop):
        piece = y_piece(arr, zz, 1 - par)
        return rcopy(piece, piece, yd_s.at[arr, side, hop], yd_r.at[arr, side, hop], sib)

    def own_copy(arr):
        piece = weights[arr].at[pl.ds(shard_at(z, c), shard)]
        return rcopy(piece, piece, wo_s.at[arr], wo_r.at[arr], sib)

    def w_first(arr):
        own_copy(arr).start()
        for k in range(ZW):
            wz_copy(arr, z, 0, jnp.int32(k), zdev(z + 1)).start()
            wz_copy(arr, z, 1, jnp.int32(k), zdev(z - 1)).start()

    def y_serve(arr, hop):
        hop = jnp.int32(hop)

        @pl.when(hop < HALF)
        def _():
            for side in range(2):
                wy_copy(arr, z, side, hop, 1 - par).wait_recv()
                yd_copy(arr, zside(side, hop), side, hop).start()

        @pl.when(hop == HALF)
        def _():
            wy_copy(arr, z, 0, hop, 1 - par).wait_recv()
            yd_copy(arr, at(z + HALF), 0, hop).start()

    def w_serve(arr, k):
        k = jnp.int32(k)
        hop = k // ZW + 1
        last_way = lax.rem(k, ZW) == 2

        @pl.when(hop < HALF)
        def _():
            for side in range(2):
                wz_copy(arr, z, side, k, zdev(z + 1)).wait_recv()

        @pl.when(hop < HALF - 1)
        def _():
            wz_copy(arr, at(z - hop), 0, k + ZW, zdev(z + 1)).start()
            wz_copy(arr, at(z + hop), 1, k + ZW, zdev(z - 1)).start()

        @pl.when(hop == HALF - 1)
        def _():
            wz_copy(arr, at(z - hop * sgn), 0, k + ZW, zdev(z + sgn)).start()

        @pl.when(hop < HALF)
        def _():
            for side in range(2):
                wd_copy(arr, zside(side, hop), side, k).start()
            if paired:
                @pl.when(last_way)
                def _():
                    for side in range(2):
                        wy_copy(arr, zside(side, hop), side, hop, par).start()

        @pl.when(hop == HALF)
        def _():
            wz_copy(arr, z, 0, k, zdev(z + 1)).wait_recv()
            wd_copy(arr, at(z + HALF), 0, k).start()
            if paired:
                pl.when(last_way)(lambda: wy_copy(arr, at(z + HALF), 0, hop, par).start())

        if arr == 0:
            pl.when(k == NP - ZW - 1)(lambda: w_first(1))
        if paired:
            pl.when((lax.rem(k, ZW) == 0) & (hop > 2))(lambda: y_serve(arr, hop - 2))

    served = [0]
    y_done = [0, 0]

    def count_y(arr, count):
        y_done[arr] = max(y_done[arr], (count - 1) // ZW - 1)

    def need_y(arr, hop):
        while paired and y_done[arr] < hop:
            y_done[arr] += 1
            y_serve(arr, y_done[arr])

    def serve(count):
        for _ in range(count):
            if served[0] == 2 * NP:
                return
            arr, k = served[0] // NP, served[0] % NP
            w_serve(arr, k)
            count_y(arr, k + 1)
            served[0] += 1
            if arr == 1 and k in (0, 2):
                need_y(0, HALF - 1 if k == 0 else HALF)

    lz_copy(z, 0, 1, zdev(z + 1)).start()
    lz_copy(z, 1, 1, zdev(z - 1)).start()
    ld_copy(z, 0, 0).start()
    for load in (loads[0], loads[1], loads[3]):
        load.wait()
    x_first(0)
    w_first(0)

    query_norm = normalize(ql[...], q_gain)
    scale = (PLAIN + ROTARY) ** (-0.5) * math.log2(math.e)
    queries = jnp.transpose(jnp.dot(query_norm, wq[...], preferred_element_type=f32) * scale)
    wide = PLAIN + ROTARY
    for h in range(HP):
        base = h * wide
        first = queries[base + PLAIN:base + PLAIN + half]
        second = queries[base + PLAIN + half:base + wide]
        qx[x, c, base:base + PLAIN, :] = queries[base:base + PLAIN].astype(bf)
        qx[x, c, base + PLAIN:base + PLAIN + half, :] = (first * cosine - second * sine).astype(bf)
        qx[x, c, base + PLAIN + half:base + wide, :] = (second * cosine + first * sine).astype(bf)
    x_first(1)
    q2t[...] = jnp.zeros_like(q2t)
    m_sc[...] = jnp.full_like(m_sc, -1e30)
    l_sc[...] = jnp.zeros_like(l_sc)
    o_sc[...] = jnp.zeros_like(o_sc)

    lz_step(1)
    loads[4].wait()
    x_relay(0)
    serve(1)
    if HALF > 2:
        lz_step(2)
        serve(1)
    x_relay(1)
    x_share(0)
    if HALF > 3:
        lz_step(3)
        serve(1)
    x_share(1)
    loads[2].wait()
    x_first(2)
    x_end(0)
    step = PLAIN + VALUE
    key_rows = []
    for jj in range(X // 2):
        by_row = jnp.transpose(WKV[c * (X // 2) + jj].astype(f32))
        for h in range(HP):
            key_rows.append(by_row[h * step:h * step + PLAIN])
            wvt[(jj * HP + h) * VALUE:(jj * HP + h + 1) * VALUE, :] = by_row[h * step + PLAIN:(h + 1) * step].astype(bf)
    wk[...] = jnp.transpose(jnp.concatenate(key_rows, axis=0)).astype(bf)
    if HALF > 4:
        lz_step(4)
        serve(2)
    x_end(1)
    for jj in range(X // 2):
        for h in range(HP):
            hc = jj * HP + h
            p, hh = hc // 2, hc % 2
            for cc in range(2):
                lanes = slice((2 * hh + cc) * T, (2 * hh + cc + 1) * T)
                q2t[p, hh * PLAIN:(hh + 1) * PLAIN, lanes] = qx[c * (X // 2) + jj, cc, h * wide:h * wide + PLAIN, :]
                q2t[p, LANES:LANES + ROTARY, lanes] = qx[c * (X // 2) + jj, cc, h * wide + PLAIN:(h + 1) * wide, :]
    begun = 4 if HALF > 4 else HALF - 1 if HALF > 2 else 1

    def attend(za, zb):
        lhs = jnp.concatenate(
            [
                jnp.concatenate(
                    [xb[zz, :, kb * share:(kb + 1) * share, :].reshape(2 * share, LANES) for zz in (za, zb)], axis=0
                )
                for kb in range(KB)
            ],
            axis=1,
        )
        rope = []
        for zz in (za, zb):
            for core in range(2):
                packed = xb[zz, core, KB * share:, :].astype(f32)
                for g in range(gsub):
                    rope.append(packed if g == 0 else pltpu.roll(packed, LANES - g * ROTARY, 1))
        rope = jnp.concatenate(rope, axis=0).astype(bf)
        kk = jnp.dot(lhs, wk[...], preferred_element_type=f32).astype(bf)
        vt = nt_dot(wvt[...], lhs).astype(bf)
        for p in range(HC // 2):
            k2 = jnp.concatenate([kk[:, p * LANES:(p + 1) * LANES], rope], axis=1)
            s_buf[p] = jnp.dot(k2, q2t[p], preferred_element_type=f32)
            old = m_sc[p:p + 1, :]
            new = jnp.maximum(old, jnp.max(s_buf[p], axis=0, keepdims=True))
            factor = jnp.exp2(old - new)
            m_sc[p:p + 1, :] = new
            expo = jnp.exp2(s_buf[p] - new)
            l_sc[p:p + 1, :] = l_sc[p:p + 1, :] * factor + jnp.sum(expo, axis=0, keepdims=True)
            weights_t = expo.astype(bf)
            for hh in range(2):
                h = 2 * p + hh
                lanes = slice(hh * 2 * T, (hh + 1) * 2 * T)
                o_sc[h] = o_sc[h] * factor[:, lanes] + jnp.dot(
                    vt[h * VALUE:(h + 1) * VALUE, :], weights_t[:, lanes], preferred_element_type=f32
                )

    base = served[0]
    rounds = HALF // 2

    def phase(u, carry):
        for s in range(2):
            t = 2 * u + 1 + s
            pl.when(t + begun <= HALF)(lambda: lz_step(t + begun))
            for n in range(2):
                k = base + 2 * (t - 1) + n
                pl.when(k < NP)(lambda: w_serve(0, k))
            if s == 0:
                pl.when(u == min(1, rounds - 1))(lambda: x_relay(2))
            else:
                pl.when(u == min(2, rounds - 1))(lambda: x_share(2))

            @pl.when(t < HALF)
            def _():
                for side in range(2):
                    ld_copy(z, side, t).wait_recv()

            @pl.when(t == HALF)
            def _():
                ld_copy(z, 0, t).wait_recv()
                ld_copy(z, 0, 0).wait_recv()

            attend(at(z - lax.rem(t, HALF)), at(z + t))
        return carry

    lax.fori_loop(0, rounds, phase, 0)
    served[0] = min(base + 2 * HALF, NP)
    count_y(0, served[0])

    heads = []
    for h in range(HC):
        p, hh = h // 2, h % 2
        heads.append(o_sc[h] / l_sc[p:p + 1, hh * 2 * T:(hh + 1) * 2 * T])
    lse[x] = jnp.zeros_like(lse[x])
    lse[x, 0:HC // 2, :] = m_sc[...] + jnp.log2(l_sc[...])
    level = [
        rcopy(lse.at[x], lse.at[x], ml_s.at[d - 1], ml_r.at[d - 1], xdev(d)) for d in range(1, X)
    ]
    for copy in level:
        copy.start()
    ours = jnp.transpose(jnp.concatenate(heads, axis=0)).astype(bf)
    for q in range(X):
        for cc in range(2):
            obuf[q, cc] = ours[cc * T + q * share:cc * T + (q + 1) * share]
    far = [rcopy(obuf.at[xat(2), i], relay.at[i], mh_s.at[i], mh_r.at[i], xdev(d)) for i, d in enumerate((1, -1))]
    near = [rcopy(obuf.at[xat(d)], orx.at[x], mo_s.at[i], mo_r.at[i], xdev(d)) for i, d in enumerate((1, -1))]
    for copy in far + near:
        copy.start()
    serve(2)
    passed = []
    for i, d in enumerate((1, -1)):
        far[i].wait_recv()
        passed.append(rcopy(relay.at[i], orx.at[xat(-d), i], mr_s.at[i], mr_r.at[i], xdev(d)))
        passed[-1].start()
    for copy in level:
        copy.wait_recv()
    top = jnp.maximum(jnp.maximum(lse[0], lse[1]), jnp.maximum(lse[2], lse[3]))
    shares = [jnp.exp2(lse[q] - top) for q in range(X)]
    norm = 1.0 / (shares[0] + shares[1] + shares[2] + shares[3])
    wts[...] = jnp.transpose(jnp.concatenate([part_of * norm for part_of in shares], axis=0))
    x_end(2)
    serve(1)
    for copy in near + passed:
        copy.wait_recv()

    def merged(cc):
        total = 0.0
        for q in range(X):
            coef = []
            for h in range(HC):
                p, hh = h // 2, h % 2
                column = wts[pl.ds(pl.multiple_of((2 * hh + cc) * T + x * share, share), share), :]
                coef.append(jnp.broadcast_to(column[:, q * 8 + p:q * 8 + p + 1], (share, VALUE)))
            source = orx[q, cc].astype(f32)
            total = total + jnp.concatenate(coef, axis=1) * source
        return total.astype(bf)

    orx[x] = obuf[x]
    width = HC * VALUE
    columns = pl.ds(pl.multiple_of(c * width, width), width)
    msend[...] = merged(1 - c)
    across = rcopy(msend, mixed.at[:, columns], md_s.at[0], md_r.at[0], sib)
    across.start()
    mixed[:, columns] = merged(c)
    serve(1)
    across.wait_recv()
    NB = 256
    for n in range(W // NB):
        cols = slice(n * NB, (n + 1) * NB)
        branch = 0.0
        for q in range(X):
            rows = HP * VALUE
            branch = branch + jnp.dot(
                mixed[:, q * rows:(q + 1) * rows], WO[q, :, cols], preferred_element_type=f32
            )
        mid[:, cols] = (hrow[:, cols].astype(f32) + branch).astype(bf)
    nb[rowsof(x), :] = normalize(mid[...], gain)
    def quarter_rows(q, i):
        return nb.at[pl.ds(pl.multiple_of(q * share + i * (share // 2), share // 2), share // 2)]

    def spread_copy(n, i, d):
        piece = quarter_rows(x, i if n == 0 else 1 - i)
        return rcopy(piece, piece, ag_s.at[n, i], ag_r.at[n, i], xdev(d))

    spread = [[spread_copy(n, i, d) for i, d in enumerate((1, -1))] for n in range(2)]
    for copy in spread[0] + spread[1]:
        copy.start()
    serve(3)
    onward = []
    for i, d in enumerate((1, -1)):
        spread[0][i].wait_recv()
        piece = quarter_rows(xat(-d), i)
        onward.append(rcopy(piece, piece, ah_s.at[i], ah_r.at[i], xdev(d)))
        onward[-1].start()
    serve(3)
    for copy in spread[1] + onward:
        copy.wait_recv()

    def wd_wait(arr, hop):
        for side in range(2 if hop < HALF else 1):
            for k in range(ZW * (hop - 1), ZW * hop):
                wd_copy(arr, z, side, jnp.int32(k)).wait_recv()
            if paired:
                yd_copy(arr, z, side, jnp.int32(hop)).wait_recv()

    while served[0] < NP:
        serve(1)
    need_y(0, HALF)
    own_copy(0).wait_recv()
    for hop in range(1, HALF + 1):
        wd_wait(0, hop)
    CUTS = 4
    per = F // NB // CUTS
    for stage in range(CUTS):
        def up(n, carry):
            cols = pl.ds(pl.multiple_of(n * NB, NB), NB)
            high = jnp.maximum(jnp.dot(nb[...], U[:, cols], preferred_element_type=f32), 0.0)
            act[:, cols] = (high * high).astype(bf)
            return carry
        lax.fori_loop(stage * per, (stage + 1) * per, up, 0)
        serve(2)

    def fa_copy(t, i, d):
        return rcopy(osend.at[t, xat(2), i], opart.at[t, i], fa_s.at[t, i], fa_r.at[t, i], xdev(d))

    def fo_copy(t, i, d):
        return rcopy(osend.at[t, xat(d)], orecv.at[t, i], fo_s.at[t, i], fo_r.at[t, i], xdev(d))

    direct = rcopy(osend.at[HALF - 1, xat(2)], ofar, fz_s.at[0], fz_r.at[0], xdev(2))

    def pair_of(t):
        return at(z - (t % HALF)), at(z + t)

    def pass_on(t):
        for i, d in enumerate((1, -1)):
            fa_copy(t, i, d).wait_recv()
            osend[t, xat(d), i] = (osend[t, xat(d), i].astype(f32) + opart[t, i].astype(f32)).astype(bf)
            fo_copy(t, i, d).start()

    for t in range(1, HALF + 1):
        while served[0] < min(NP + ZW * (t + 1) + 1, 2 * NP):
            serve(1)
        need_y(1, t)
        if t == HALF:
            own_copy(1).wait_recv()
        wd_wait(1, t)
        rhs = jnp.concatenate(
            [D[pl.ds(pl.multiple_of(zz * 2 * shard, 2 * shard), 2 * shard), :] for zz in pair_of(t)], axis=0
        )
        block = nt_dot(act[...], rhs).astype(bf)
        for q in range(X):
            for side in range(2):
                osend[t - 1, q, side] = block[q * share:(q + 1) * share, side * LANES:(side + 1) * LANES]
        if t < HALF:
            for i, d in enumerate((1, -1)):
                fa_copy(t - 1, i, d).start()
        else:
            direct.start()
            for i, d in enumerate((1, -1)):
                fo_copy(t - 1, i, d).start()
        if t > 1:
            pass_on(t - 2)
    for t in range(1, HALF + 1):
        for i, d in enumerate((1, -1)):
            fo_copy(t - 1, i, d).wait_recv()
        if t == HALF:
            direct.wait_recv()
        for side, zz in enumerate(pair_of(t)):
            cols = pl.ds(pl.multiple_of(zz * LANES, LANES), LANES)
            total = osend[t - 1, x, side].astype(f32)
            for i in range(2):
                total = total + orecv[t - 1, i, side].astype(f32)
            if t == HALF:
                total = total + ofar[side].astype(f32)
            out[:, cols] = (mid[:, cols].astype(f32) + total).astype(bf)

    for copy in level + far + near + passed + [across] + spread[0] + spread[1] + onward + [ld_copy(z, 0, 0), own_copy(0), own_copy(1)]:
        copy.wait_send()
    for t in range(HALF):
        for i, d in enumerate((1, -1)):
            if t < HALF - 1:
                fa_copy(t, i, d).wait_send()
            fo_copy(t, i, d).wait_send()
    direct.wait_send()
    for what in range(3):
        for i, d in enumerate((1, -1)):
            x1_copy(what, i, d).wait_send()
            x2_copy(what, i, d).wait_send()
        for n in range(X - 1 if what == 2 else X // 2):
            if what == 0:
                pl.when((1 - c) * (X // 2) + n != x)(lambda: xd_copy(0, n).wait_send())
            else:
                xd_copy(what, n).wait_send()

    def drain(t, carry):
        def one(side):
            lz_copy(z, side, t, zdev(z + 1)).wait_send()
            ld_copy(z, side, t).wait_send()
            for arr in range(2):
                for s in range(ZW):
                    wz_copy(arr, z, side, ZW * (t - 1) + s, zdev(z + 1)).wait_send()
                    wd_copy(arr, z, side, ZW * (t - 1) + s).wait_send()
                if paired:
                    wy_copy(arr, z, side, t, par).wait_send()
                    yd_copy(arr, z, side, t).wait_send()
        one(0)
        pl.when(t < HALF)(lambda: one(1))
        return carry
    lax.fori_loop(1, HALF + 1, drain, 0)


def fused_layer(Z, X, paired, kvl, key_t, up_own, dn_own, hid, ql, wq, wkv, wo, cos_t, sin_t, q_gain, kv_gain, gain):
    HALF = Z // 2
    T, W = hid.shape
    F = up_own.shape[1]
    share = T // X
    rows = kvl.shape[1] // LANES * share + share * ROTARY // LANES
    bf, f32 = jnp.bfloat16, jnp.float32
    DMA = pltpu.SemaphoreType.DMA
    any_ = pl.BlockSpec(memory_space=pl.ANY)
    vm = pl.BlockSpec(memory_space=pltpu.VMEM)
    R = kvl.shape[1]
    hc = wkv.shape[1] // (PLAIN + VALUE) * X // 2
    scratch = [
        pltpu.VMEM((Z, 2, rows, LANES), bf),
        pltpu.VMEM((T, LANES), f32),
        pltpu.VMEM((W, F), bf),
        pltpu.VMEM((W, F), bf),
        pltpu.VMEM((share, W), bf),
        pltpu.VMEM((X,) + wkv.shape, bf),
        pltpu.VMEM((X,) + wo.shape, bf),
        pltpu.VMEM((X, 2, wq.shape[1], T), bf),
        pltpu.VMEM((hc // 2, 2 * LANES, 4 * T), bf),
        pltpu.VMEM((R, hc * PLAIN), bf),
        pltpu.VMEM((hc * VALUE, R), bf),
        pltpu.VMEM((hc // 2, 4 * share, 4 * T), f32),
        pltpu.VMEM((hc // 2, 4 * T), f32),
        pltpu.VMEM((hc // 2, 4 * T), f32),
        pltpu.VMEM((hc, VALUE, 2 * T), f32),
        pltpu.VMEM((X, 2, share, hc * VALUE), bf),
        pltpu.VMEM((X, 2, share, hc * VALUE), bf),
        pltpu.VMEM((2, share, hc * VALUE), bf),
        pltpu.VMEM((X, 8, 4 * T), f32),
        pltpu.VMEM((4 * T, X * 8), f32),
        pltpu.VMEM((share, hc * VALUE), bf),
        pltpu.VMEM((share, 2 * hc * VALUE), bf),
        pltpu.VMEM((share, W), bf),
        pltpu.VMEM((T, W), bf),
        pltpu.VMEM((T, F), bf),
        pltpu.VMEM((HALF, X, 2, share, LANES), bf),
        pltpu.VMEM((HALF, 2, 2, share, LANES), bf),
        pltpu.VMEM((HALF, 2, share, LANES), bf),
        pltpu.VMEM((2, share, LANES), bf),
        DMA((5,)),
    ]
    for shape in (
        (2, HALF + 1), (2, HALF + 1),
        (2, 2, 4 * HALF), (2, 2, HALF + 1), (2, 2, 4 * HALF), (2, 2, HALF + 1), (2,),
        (3, 2), (3, 2), (3, X - 1), (X - 1,), (2,), (2,), (2,), (1,),
        (2, 2), (2,), (HALF, 2), (HALF, 2), (1,),
    ):
        scratch += [DMA(shape), DMA(shape)]
    return pl.pallas_call(
        functools.partial(layer_kernel, Z, X, paired),
        out_shape=jax.ShapeDtypeStruct((share, W), bf),
        in_specs=[vm, vm, any_, any_, any_, vm, vm, any_, any_] + [vm] * 5,
        out_specs=vm,
        scratch_shapes=scratch,
        compiler_params=pltpu.CompilerParams(
            collective_id=0, has_side_effects=True, vmem_limit_bytes=62 * 1024 * 1024
        ),
        name="layer",
    )(kvl, key_t, up_own, dn_own, hid, ql, wq, wkv, wo, cos_t, sin_t, q_gain, kv_gain, gain)


def on_device(
    hidden_in, query_latent_rows, key_value_latent, rotary_key, query_norm_gain, key_value_gain,
    query_up_weight, key_value_up_weight, out_proj, feed_gain, feed_up, feed_down,
):
    X = lax.axis_size("tp")
    Z = lax.axis_size("sp") // 2
    paired = lax.axis_size("grp") % 2 == 0
    T = hidden_in.shape[0]
    half = ROTARY // 2
    position = (lax.axis_index("sp") * T + jnp.arange(T)).astype(jnp.float32)
    inverse = 10000.0 ** (-jnp.arange(half, dtype=jnp.float32) * 2.0 / ROTARY)
    angles = inverse[:, None] * position[None, :]
    return fused_layer(
        Z, X, paired, key_value_latent, rotary_key.T, feed_up, feed_down.T, hidden_in, query_latent_rows,
        query_up_weight, key_value_up_weight, out_proj, jnp.cos(angles), jnp.sin(angles),
        query_norm_gain.reshape(-1, LANES), key_value_gain.reshape(-1, LANES), feed_gain.reshape(-1, LANES),
    )


def solution(mesh):
    return jax.shard_map(
        on_device,
        mesh=mesh,
        in_specs=(
            P(("grp", "sp"), None),
            P(("grp", "sp"), None),
            P(("grp", "sp"), None),
            P(("grp", "sp"), None),
            P(),
            P(),
            P(None, "tp"),
            P(None, "tp"),
            P("tp", None),
            P(),
            P("sp", "tp"),
            P("tp", "sp"),
        ),
        out_specs=P(("grp", "sp", "tp"), None),
        check_vma=False,
    )
```

time: 172 us -> 152 us (0.88)
  Pallas kernels: 162 us -> 149 us
  local copies, waits for them, and re-layouts: 6.52 us -> 1.67 us
  other arithmetic: 3.15 us -> 0.77 us
    pallas_call x1, Pallas kernels: 162 us -> 149 us  [fused_layer(): pl.pallas_call(functools.partial(layer_kernel, Z, X, paired), out_shape=j...]
    unnamed x16 -> x1, local copies, waits for them, and re-layouts: 3.39 us -> 1.67 us
where the time goes in v2:
time: 152 us
  Pallas kernels  149 us (98%)
  local copies, waits for them, and re-layouts  1.67 us (1%)
    pallas_call x1, Pallas kernels, fused_layer(): pl.pallas_call(functools.partial(layer_kernel, Z, X, paired), out_shape=j...  149 us

profile of v2, /device:TPU:33, one launch (start us, length us, event | category | flops | bytes accessed | tf_op | source)
XLA Modules:
  0.0 151.7 jit_solution(3065357660439453796)
XLA Ops:
  0.0 0.8 multiply_sine_fusion
  0.8 149.2 %layer.1 = bf16[64,2048]{1,0:T(8,128)(2,1)} custom-call(bf16[256,512]{1,0:T(8,128)(2,1)} %kvl.1, bf16[32,256]{1,0:T(8,128)(2,1)} %bitcast.6, bf16[64,2048]{1,0:T(8,128)(2,1)} %up_own.1, bf16[64,2048]{1,0:T(8,128)(2,1)} %bitcast.5, bf16[256,2048]{1,0:T(8,128)(2,1)} %hid.1, bf16[256,768]{1,0:T(8,128)(2,1)} %ql.1, bf16[768,384]{1,0:T(8,128)(2,1)} %wq.1, ...), custom_call_target="tpu_custom_call" | custom-call | tf_op jit(solution)/shard_map/layer/pallas_call | solution.py:719
  150.0 1.7 %copy.14 = bf16[64,2048]{1,0:T(8,128)(2,1)} copy(bf16[64,2048]{1,0:T(8,128)(2,1)} %layer.1) | data formatting | bytes 524288
  (2 shorter events, 0.0 us)

commit v3 on v2

--- a/solution.py
+++ b/solution.py
@@ -35,10 +35,10 @@
     Z, X, paired,
     kvl, key_t, up_own, dn_own, hid, ql, wq, wkv, wo, cos_t, sin_t, q_gain, kv_gain, gain,
     out,
-    xb, turned_key, U, D, hrow, WKV, WO, qx, q2t, wk, wvt, s_buf, m_sc, l_sc, o_sc, obuf, orx, relay, lse, wts, msend, mixed,
+    xb, turned_key, U, D, hrow, WKV, WO, qx, q2t, wk, wvt, s_buf, m_sc, l_sc, o_sc, obuf, orx, relay, lse, lrx, wts, mixed,
     mid, nb, act, osend, orecv, opart, ofar,
-    loc_s, lz_s, lz_r, ld_s, ld_r, wz_s, wz_r, wy_s, wy_r, wd_s, wd_r, yd_s, yd_r, wo_s, wo_r,
-    x1_s, x1_r, x2_s, x2_r, xd_s, xd_r, ml_s, ml_r, mo_s, mo_r, mh_s, mh_r, mr_s, mr_r, md_s, md_r,
+    loc_s, lz_s, lz_r, ld_s, ld_r, w_s, wz_r, wy_r, wd_r,
+    x1_s, x1_r, x2_s, x2_r, xd_s, xd_r, ml_s, ml_r, mo_s, mo_r, mh_s, mh_r,
     ag_s, ag_r, ah_s, ah_r, fa_s, fa_r, fo_s, fo_r, fz_s, fz_r,
 ):
     HALF = Z // 2
@@ -100,7 +100,8 @@
     for load in loads:
         load.start()
     barrier = pltpu.get_barrier_semaphore()
-    peers = [zdev(z + 1), zdev(z - 1), sib] + [xdev(d) for d in range(1, X)] + ([twin] if paired else [])
+    peers = [zdev(z + 1), zdev(z - 1), sib] + ([twin] if paired else [])
+    peers += [{"sp": 2 * z + core, "tp": xat(d)} for d in range(1, X) for core in range(2)]
     for dev in peers:
         pl.semaphore_signal(barrier, inc=1, device_id=dev, device_id_type=MESH)
 
@@ -128,39 +129,45 @@
     xb[z, c, KB * share:, :] = packed_key.astype(bf)
     pl.semaphore_wait(barrier, len(peers))
 
-    def lz_copy(zz, side, hop, dev):
+    def lz_copy(zz, hop, dev):
         piece = xb.at[zz, c]
-        return rcopy(piece, piece, lz_s.at[side, hop], lz_r.at[side, hop], dev)
-
-    def ld_copy(zz, side, t):
-        return rcopy(xb.at[zz, c], xb.at[zz, c], ld_s.at[side, t], ld_r.at[side, t], sib)
+        return rcopy(piece, piece, lz_s.at[0], lz_r.at[hop], dev)
+
+    def ld_copy(zz, t):
+        return rcopy(xb.at[zz, c], xb.at[zz, c], ld_s.at[0], ld_r.at[t], sib)
+
+    def lz_wait(hop, count):
+        pieces = xb.at[pl.ds(0, count), 0]
+        rcopy(pieces, pieces, lz_s.at[0], lz_r.at[hop], sib).wait_recv()
+
+    def ld_wait(t):
+        rcopy(xb.at[0], xb.at[0], ld_s.at[0], ld_r.at[t], sib).wait_recv()
 
     def lz_step(i):
         i = jnp.int32(i)
 
         @pl.when(i < HALF)
         def _():
+            lz_wait(i, 2)
+
+        @pl.when(i < HALF - 1)
+        def _():
+            lz_copy(at(z - i), i + 1, zdev(z + 1)).start()
+            lz_copy(at(z + i), i + 1, zdev(z - 1)).start()
+
+        @pl.when(i == HALF - 1)
+        def _():
+            lz_copy(at(z - i * sgn), i + 1, zdev(z + sgn)).start()
+
+        @pl.when(i < HALF)
+        def _():
             for side in range(2):
-                lz_copy(z, side, i, zdev(z + 1)).wait_recv()
-
-        @pl.when(i < HALF - 1)
-        def _():
-            lz_copy(at(z - i), 0, i + 1, zdev(z + 1)).start()
-            lz_copy(at(z + i), 1, i + 1, zdev(z - 1)).start()
-
-        @pl.when(i == HALF - 1)
-        def _():
-            lz_copy(at(z - i * sgn), 0, i + 1, zdev(z + sgn)).start()
-
-        @pl.when(i < HALF)
-        def _():
-            for side in range(2):
-                ld_copy(zside(side, i), side, i).start()
+                ld_copy(zside(side, i), i).start()
 
         @pl.when(i == HALF)
         def _():
-            lz_copy(z, 0, i, zdev(z + 1)).wait_recv()
-            ld_copy(at(z + HALF), 0, i).start()
+            lz_wait(i, 1)
+            ld_copy(at(z + HALF), i).start()
 
     kv_half, q_half, o_half = WKV.shape[1] // 2, qx.shape[2], WO.shape[1] // 2
 
@@ -229,45 +236,45 @@
     def y_piece(arr, zz, turn):
         return weights[arr].at[place(zz, 2 + turn)]
 
-    def wz_copy(arr, zz, side, k, dev):
+    def wz_copy(arr, zz, k, dev):
         piece = z_piece(arr, zz, k)
-        return rcopy(piece, piece, wz_s.at[arr, side, k], wz_r.at[arr, side, k], dev)
-
-    def wy_copy(arr, zz, side, hop, turn):
+        return rcopy(piece, piece, w_s.at[0], wz_r.at[arr, k], dev)
+
+    def wy_copy(arr, zz, hop, turn):
         piece = y_piece(arr, zz, turn)
-        return rcopy(piece, piece, wy_s.at[arr, side, hop], wy_r.at[arr, side, hop], twin)
-
-    def wd_copy(arr, zz, side, k):
-        piece = z_piece(arr, zz, k)
-        return rcopy(piece, piece, wd_s.at[arr, side, k], wd_r.at[arr, side, k], sib)
-
-    def yd_copy(arr, zz, side, hop):
-        piece = y_piece(arr, zz, 1 - par)
-        return rcopy(piece, piece, yd_s.at[arr, side, hop], yd_r.at[arr, side, hop], sib)
-
-    def own_copy(arr):
-        piece = weights[arr].at[pl.ds(shard_at(z, c), shard)]
-        return rcopy(piece, piece, wo_s.at[arr], wo_r.at[arr], sib)
+        return rcopy(piece, piece, w_s.at[0], wy_r.at[arr, hop], twin)
+
+    def to_sib(arr, piece, hop):
+        return rcopy(piece, piece, w_s.at[1], wd_r.at[0 if arr == 0 else hop], sib)
+
+    def w_rows(count):
+        return weights[0].at[pl.ds(0, count)]
+
+    def wz_wait(arr, k, count):
+        rcopy(w_rows(count * part), w_rows(count * part), w_s.at[0], wz_r.at[arr, k], sib).wait_recv()
+
+    def wy_wait(arr, hop, count):
+        rcopy(w_rows(count * part), w_rows(count * part), w_s.at[0], wy_r.at[arr, hop], sib).wait_recv()
 
     def w_first(arr):
-        own_copy(arr).start()
+        to_sib(arr, weights[arr].at[pl.ds(shard_at(z, c), shard)], HALF).start()
         for k in range(ZW):
-            wz_copy(arr, z, 0, jnp.int32(k), zdev(z + 1)).start()
-            wz_copy(arr, z, 1, jnp.int32(k), zdev(z - 1)).start()
+            wz_copy(arr, z, jnp.int32(k), zdev(z + 1)).start()
+            wz_copy(arr, z, jnp.int32(k), zdev(z - 1)).start()
 
     def y_serve(arr, hop):
         hop = jnp.int32(hop)
 
         @pl.when(hop < HALF)
         def _():
+            wy_wait(arr, hop, 2)
             for side in range(2):
-                wy_copy(arr, z, side, hop, 1 - par).wait_recv()
-                yd_copy(arr, zside(side, hop), side, hop).start()
+                to_sib(arr, y_piece(arr, zside(side, hop), 1 - par), hop).start()
 
         @pl.when(hop == HALF)
         def _():
-            wy_copy(arr, z, 0, hop, 1 - par).wait_recv()
-            yd_copy(arr, at(z + HALF), 0, hop).start()
+            wy_wait(arr, hop, 1)
+            to_sib(arr, y_piece(arr, at(z + HALF), 1 - par), hop).start()
 
     def w_serve(arr, k):
         k = jnp.int32(k)
@@ -276,34 +283,33 @@
 
         @pl.when(hop < HALF)
         def _():
+            wz_wait(arr, k, 2)
+
+        @pl.when(hop < HALF - 1)
+        def _():
+            wz_copy(arr, at(z - hop), k + ZW, zdev(z + 1)).start()
+            wz_copy(arr, at(z + hop), k + ZW, zdev(z - 1)).start()
+
+        @pl.when(hop == HALF - 1)
+        def _():
+            wz_copy(arr, at(z - hop * sgn), k + ZW, zdev(z + sgn)).start()
+
+        @pl.when(hop < HALF)
+        def _():
             for side in range(2):
-                wz_copy(arr, z, side, k, zdev(z + 1)).wait_recv()
-
-        @pl.when(hop < HALF - 1)
-        def _():
-            wz_copy(arr, at(z - hop), 0, k + ZW, zdev(z + 1)).start()
-            wz_copy(arr, at(z + hop), 1, k + ZW, zdev(z - 1)).start()
-
-        @pl.when(hop == HALF - 1)
-        def _():
-            wz_copy(arr, at(z - hop * sgn), 0, k + ZW, zdev(z + sgn)).start()
-
-        @pl.when(hop < HALF)
-        def _():
-            for side in range(2):
-                wd_copy(arr, zside(side, hop), side, k).start()
+                to_sib(arr, z_piece(arr, zside(side, hop), k), hop).start()
             if paired:
                 @pl.when(last_way)
                 def _():
                     for side in range(2):
-                        wy_copy(arr, zside(side, hop), side, hop, par).start()
+                        wy_copy(arr, zside(side, hop), hop, par).start()
 
         @pl.when(hop == HALF)
         def _():
-            wz_copy(arr, z, 0, k, zdev(z + 1)).wait_recv()
-            wd_copy(arr, at(z + HALF), 0, k).start()
+            wz_wait(arr, k, 1)
+            to_sib(arr, z_piece(arr, at(z + HALF), k), hop).start()
             if paired:
-                pl.when(last_way)(lambda: wy_copy(arr, at(z + HALF), 0, hop, par).start())
+                pl.when(last_way)(lambda: wy_copy(arr, at(z + HALF), hop, par).start())
 
         if arr == 0:
             pl.when(k == NP - ZW - 1)(lambda: w_first(1))
@@ -332,9 +338,9 @@
             if arr == 1 and k in (0, 2):
                 need_y(0, HALF - 1 if k == 0 else HALF)
 
-    lz_copy(z, 0, 1, zdev(z + 1)).start()
-    lz_copy(z, 1, 1, zdev(z - 1)).start()
-    ld_copy(z, 0, 0).start()
+    lz_copy(z, 1, zdev(z + 1)).start()
+    lz_copy(z, 1, zdev(z - 1)).start()
+    ld_copy(z, HALF).start()
     for load in (loads[0], loads[1], loads[3]):
         load.wait()
     x_first(0)
@@ -381,8 +387,7 @@
             key_rows.append(by_row[h * step:h * step + PLAIN])
             wvt[(jj * HP + h) * VALUE:(jj * HP + h + 1) * VALUE, :] = by_row[h * step + PLAIN:(h + 1) * step].astype(bf)
     wk[...] = jnp.transpose(jnp.concatenate(key_rows, axis=0)).astype(bf)
-    if HALF > 4:
-        lz_step(4)
+    if HALF > 3:
         serve(2)
     x_end(1)
     for jj in range(X // 2):
@@ -393,7 +398,7 @@
                 lanes = slice((2 * hh + cc) * T, (2 * hh + cc + 1) * T)
                 q2t[p, hh * PLAIN:(hh + 1) * PLAIN, lanes] = qx[c * (X // 2) + jj, cc, h * wide:h * wide + PLAIN, :]
                 q2t[p, LANES:LANES + ROTARY, lanes] = qx[c * (X // 2) + jj, cc, h * wide + PLAIN:(h + 1) * wide, :]
-    begun = 4 if HALF > 4 else HALF - 1 if HALF > 2 else 1
+    begun = 3 if HALF > 3 else HALF - 1 if HALF > 2 else 1
 
     def attend(za, zb):
         lhs = jnp.concatenate(
@@ -446,16 +451,7 @@
             else:
                 pl.when(u == min(2, rounds - 1))(lambda: x_share(2))
 
-            @pl.when(t < HALF)
-            def _():
-                for side in range(2):
-                    ld_copy(z, side, t).wait_recv()
-
-            @pl.when(t == HALF)
-            def _():
-                ld_copy(z, 0, t).wait_recv()
-                ld_copy(z, 0, 0).wait_recv()
-
+            ld_wait(t)
             attend(at(z - lax.rem(t, HALF)), at(z + t))
         return carry
 
@@ -467,59 +463,71 @@
     for h in range(HC):
         p, hh = h // 2, h % 2
         heads.append(o_sc[h] / l_sc[p:p + 1, hh * 2 * T:(hh + 1) * 2 * T])
-    lse[x] = jnp.zeros_like(lse[x])
-    lse[x, 0:HC // 2, :] = m_sc[...] + jnp.log2(l_sc[...])
+    final = m_sc[...] + jnp.log2(l_sc[...])
+    for cc in range(2):
+        lse[cc] = jnp.concatenate(
+            [
+                final[h // 2:h // 2 + 1, (2 * (h % 2) + cc) * T:(2 * (h % 2) + cc + 1) * T]
+                for h in range(HC)
+            ],
+            axis=0,
+        )
+    here = 2 * x + c
+
+    def owner(d, core):
+        return {"sp": 2 * z + core, "tp": xat(d)}
+
     level = [
-        rcopy(lse.at[x], lse.at[x], ml_s.at[d - 1], ml_r.at[d - 1], xdev(d)) for d in range(1, X)
+        rcopy(lse.at[cc], lrx.at[here], ml_s.at[0], ml_r.at[0], owner(d, cc)) for d in range(1, X) for cc in range(2)
     ]
+    level.append(rcopy(lse.at[1 - c], lrx.at[here], ml_s.at[0], ml_r.at[0], sib))
     for copy in level:
         copy.start()
+    lrx[here] = lse[c]
     ours = jnp.transpose(jnp.concatenate(heads, axis=0)).astype(bf)
     for q in range(X):
         for cc in range(2):
             obuf[q, cc] = ours[cc * T + q * share:cc * T + (q + 1) * share]
     far = [rcopy(obuf.at[xat(2), i], relay.at[i], mh_s.at[i], mh_r.at[i], xdev(d)) for i, d in enumerate((1, -1))]
-    near = [rcopy(obuf.at[xat(d)], orx.at[x], mo_s.at[i], mo_r.at[i], xdev(d)) for i, d in enumerate((1, -1))]
+    near = [
+        rcopy(obuf.at[xat(d), cc], orx.at[here], mo_s.at[0], mo_r.at[0], owner(d, cc))
+        for d in (1, -1) for cc in range(2)
+    ]
+    near.append(rcopy(obuf.at[x, 1 - c], orx.at[here], mo_s.at[0], mo_r.at[0], sib))
     for copy in far + near:
         copy.start()
-    serve(2)
-    passed = []
+    orx[here] = obuf[x, c]
+    serve(3)
     for i, d in enumerate((1, -1)):
         far[i].wait_recv()
-        passed.append(rcopy(relay.at[i], orx.at[xat(-d), i], mr_s.at[i], mr_r.at[i], xdev(d)))
-        passed[-1].start()
-    for copy in level:
-        copy.wait_recv()
-    top = jnp.maximum(jnp.maximum(lse[0], lse[1]), jnp.maximum(lse[2], lse[3]))
-    shares = [jnp.exp2(lse[q] - top) for q in range(X)]
-    norm = 1.0 / (shares[0] + shares[1] + shares[2] + shares[3])
-    wts[...] = jnp.transpose(jnp.concatenate([part_of * norm for part_of in shares], axis=0))
+        rcopy(relay.at[i], orx.at[2 * xat(-d) + c], mo_s.at[0], mo_r.at[0], owner(d, i)).start()
+    others = 2 * X - 1
+
+    def seven(ref, ss, rs):
+        return rcopy(ref.at[pl.ds(0, others)], ref.at[pl.ds(0, others)], ss.at[0], rs.at[0], sib)
+
+    seven(lrx, ml_s, ml_r).wait_recv()
+    coefs = []
+    for core in range(2):
+        levels = [lrx[2 * q + core] for q in range(X)]
+        top = functools.reduce(jnp.maximum, levels)
+        parts = [jnp.exp2(level_of - top) for level_of in levels]
+        norm = 1.0 / functools.reduce(jnp.add, parts)
+        coefs += [part_of * norm for part_of in parts]
+    wts[...] = jnp.transpose(jnp.concatenate(coefs, axis=0))
     x_end(2)
-    serve(1)
-    for copy in near + passed:
-        copy.wait_recv()
-
-    def merged(cc):
+    serve(3)
+    seven(orx, mo_s, mo_r).wait_recv()
+    columns = wts[rowsof(x), :]
+    for core in range(2):
         total = 0.0
         for q in range(X):
-            coef = []
-            for h in range(HC):
-                p, hh = h // 2, h % 2
-                column = wts[pl.ds(pl.multiple_of((2 * hh + cc) * T + x * share, share), share), :]
-                coef.append(jnp.broadcast_to(column[:, q * 8 + p:q * 8 + p + 1], (share, VALUE)))
-            source = orx[q, cc].astype(f32)
-            total = total + jnp.concatenate(coef, axis=1) * source
-        return total.astype(bf)
-
-    orx[x] = obuf[x]
-    width = HC * VALUE
-    columns = pl.ds(pl.multiple_of(c * width, width), width)
-    msend[...] = merged(1 - c)
-    across = rcopy(msend, mixed.at[:, columns], md_s.at[0], md_r.at[0], sib)
-    across.start()
-    mixed[:, columns] = merged(c)
-    serve(1)
-    across.wait_recv()
+            first = (core * X + q) * HC
+            coef = jnp.concatenate(
+                [jnp.broadcast_to(columns[:, first + h:first + h + 1], (share, VALUE)) for h in range(HC)], axis=1
+            )
+            total = total + coef * orx[2 * q + core].astype(f32)
+        mixed[:, core * HC * VALUE:(core + 1) * HC * VALUE] = total.astype(bf)
     NB = 256
     for n in range(W // NB):
         cols = slice(n * NB, (n + 1) * NB)
@@ -541,30 +549,24 @@
     spread = [[spread_copy(n, i, d) for i, d in enumerate((1, -1))] for n in range(2)]
     for copy in spread[0] + spread[1]:
         copy.start()
-    serve(3)
+    serve(4)
     onward = []
     for i, d in enumerate((1, -1)):
         spread[0][i].wait_recv()
         piece = quarter_rows(xat(-d), i)
         onward.append(rcopy(piece, piece, ah_s.at[i], ah_r.at[i], xdev(d)))
         onward[-1].start()
-    serve(3)
+    serve(4)
     for copy in spread[1] + onward:
         copy.wait_recv()
 
-    def wd_wait(arr, hop):
-        for side in range(2 if hop < HALF else 1):
-            for k in range(ZW * (hop - 1), ZW * hop):
-                wd_copy(arr, z, side, jnp.int32(k)).wait_recv()
-            if paired:
-                yd_copy(arr, z, side, jnp.int32(hop)).wait_recv()
+    def wd_wait(arr, hop, count):
+        rcopy(w_rows(count), w_rows(count), w_s.at[1], wd_r.at[0 if arr == 0 else hop], sib).wait_recv()
 
     while served[0] < NP:
         serve(1)
     need_y(0, HALF)
-    own_copy(0).wait_recv()
-    for hop in range(1, HALF + 1):
-        wd_wait(0, hop)
+    wd_wait(0, 0, Z * shard)
     CUTS = 4
     per = F // NB // CUTS
     for stage in range(CUTS):
@@ -574,13 +576,13 @@
             act[:, cols] = (high * high).astype(bf)
             return carry
         lax.fori_loop(stage * per, (stage + 1) * per, up, 0)
-        serve(2)
+        serve(1)
 
     def fa_copy(t, i, d):
-        return rcopy(osend.at[t, xat(2), i], opart.at[t, i], fa_s.at[t, i], fa_r.at[t, i], xdev(d))
+        return rcopy(osend.at[t, xat(2), i], opart.at[t, i], fa_s.at[0], fa_r.at[t], xdev(d))
 
     def fo_copy(t, i, d):
-        return rcopy(osend.at[t, xat(d)], orecv.at[t, i], fo_s.at[t, i], fo_r.at[t, i], xdev(d))
+        return rcopy(osend.at[t, xat(d)], orecv.at[t, i], fo_s.at[0], fo_r.at[0], xdev(d))
 
     direct = rcopy(osend.at[HALF - 1, xat(2)], ofar, fz_s.at[0], fz_r.at[0], xdev(2))
 
@@ -588,8 +590,8 @@
         return at(z - (t % HALF)), at(z + t)
 
     def pass_on(t):
+        rcopy(opart.at[t], opart.at[t], fa_s.at[0], fa_r.at[t], sib).wait_recv()
         for i, d in enumerate((1, -1)):
-            fa_copy(t, i, d).wait_recv()
             osend[t, xat(d), i] = (osend[t, xat(d), i].astype(f32) + opart[t, i].astype(f32)).astype(bf)
             fo_copy(t, i, d).start()
 
@@ -597,9 +599,7 @@
         while served[0] < min(NP + ZW * (t + 1) + 1, 2 * NP):
             serve(1)
         need_y(1, t)
-        if t == HALF:
-            own_copy(1).wait_recv()
-        wd_wait(1, t)
+        wd_wait(1, t, 2 * shard)
         rhs = jnp.concatenate(
             [D[pl.ds(pl.multiple_of(zz * 2 * shard, 2 * shard), 2 * shard), :] for zz in pair_of(t)], axis=0
         )
@@ -616,11 +616,9 @@
                 fo_copy(t - 1, i, d).start()
         if t > 1:
             pass_on(t - 2)
+    rcopy(orecv, orecv, fo_s.at[0], fo_r.at[0], sib).wait_recv()
+    direct.wait_recv()
     for t in range(1, HALF + 1):
-        for i, d in enumerate((1, -1)):
-            fo_copy(t - 1, i, d).wait_recv()
-        if t == HALF:
-            direct.wait_recv()
         for side, zz in enumerate(pair_of(t)):
             cols = pl.ds(pl.multiple_of(zz * LANES, LANES), LANES)
             total = osend[t - 1, x, side].astype(f32)
@@ -630,14 +628,13 @@
                 total = total + ofar[side].astype(f32)
             out[:, cols] = (mid[:, cols].astype(f32) + total).astype(bf)
 
-    for copy in level + far + near + passed + [across] + spread[0] + spread[1] + onward + [ld_copy(z, 0, 0), own_copy(0), own_copy(1)]:
+    for copy in far + spread[0] + spread[1] + onward + [direct]:
         copy.wait_send()
-    for t in range(HALF):
-        for i, d in enumerate((1, -1)):
-            if t < HALF - 1:
-                fa_copy(t, i, d).wait_send()
-            fo_copy(t, i, d).wait_send()
-    direct.wait_send()
+    seven(lrx, ml_s, ml_r).wait_send()
+    seven(orx, mo_s, mo_r).wait_send()
+    sent = opart.at[pl.ds(0, HALF - 1)]
+    rcopy(sent, sent, fa_s.at[0], fa_r.at[0], sib).wait_send()
+    rcopy(orecv, orecv, fo_s.at[0], fo_r.at[0], sib).wait_send()
     for what in range(3):
         for i, d in enumerate((1, -1)):
             x1_copy(what, i, d).wait_send()
@@ -647,22 +644,14 @@
                 pl.when((1 - c) * (X // 2) + n != x)(lambda: xd_copy(0, n).wait_send())
             else:
                 xd_copy(what, n).wait_send()
-
-    def drain(t, carry):
-        def one(side):
-            lz_copy(z, side, t, zdev(z + 1)).wait_send()
-            ld_copy(z, side, t).wait_send()
-            for arr in range(2):
-                for s in range(ZW):
-                    wz_copy(arr, z, side, ZW * (t - 1) + s, zdev(z + 1)).wait_send()
-                    wd_copy(arr, z, side, ZW * (t - 1) + s).wait_send()
-                if paired:
-                    wy_copy(arr, z, side, t, par).wait_send()
-                    yd_copy(arr, z, side, t).wait_send()
-        one(0)
-        pl.when(t < HALF)(lambda: one(1))
-        return carry
-    lax.fori_loop(1, HALF + 1, drain, 0)
+    sent = xb.at[pl.ds(0, Z - 1), 0]
+    rcopy(sent, sent, lz_s.at[0], lz_r.at[0], sib).wait_send()
+    sent = xb.at[pl.ds(0, HALF)]
+    rcopy(sent, sent, ld_s.at[0], ld_r.at[0], sib).wait_send()
+    sent = w_rows(2 * (Z - 1) * 4 * part)
+    rcopy(sent, sent, w_s.at[0], wz_r.at[0, 0], sib).wait_send()
+    sent = w_rows(2 * Z * shard)
+    rcopy(sent, sent, w_s.at[1], wd_r.at[0], sib).wait_send()
 
 
 def fused_layer(Z, X, paired, kvl, key_t, up_own, dn_own, hid, ql, wq, wkv, wo, cos_t, sin_t, q_gain, kv_gain, gain):
@@ -694,11 +683,11 @@
         pltpu.VMEM((hc // 2, 4 * T), f32),
         pltpu.VMEM((hc, VALUE, 2 * T), f32),
         pltpu.VMEM((X, 2, share, hc * VALUE), bf),
-        pltpu.VMEM((X, 2, share, hc * VALUE), bf),
+        pltpu.VMEM((X * 2, share, hc * VALUE), bf),
         pltpu.VMEM((2, share, hc * VALUE), bf),
-        pltpu.VMEM((X, 8, 4 * T), f32),
-        pltpu.VMEM((4 * T, X * 8), f32),
-        pltpu.VMEM((share, hc * VALUE), bf),
+        pltpu.VMEM((2, hc, T), f32),
+        pltpu.VMEM((X * 2, hc, T), f32),
+        pltpu.VMEM((T, X * 2 * hc), f32),
         pltpu.VMEM((share, 2 * hc * VALUE), bf),
         pltpu.VMEM((share, W), bf),
         pltpu.VMEM((T, W), bf),
@@ -710,12 +699,12 @@
         DMA((5,)),
     ]
     for shape in (
-        (2, HALF + 1), (2, HALF + 1),
-        (2, 2, 4 * HALF), (2, 2, HALF + 1), (2, 2, 4 * HALF), (2, 2, HALF + 1), (2,),
-        (3, 2), (3, 2), (3, X - 1), (X - 1,), (2,), (2,), (2,), (1,),
-        (2, 2), (2,), (HALF, 2), (HALF, 2), (1,),
+        (1,), (HALF + 1,), (1,), (HALF + 1,),
+        (2,), (2, 4 * HALF if not paired else 3 * HALF), (2, HALF + 1), (HALF + 1,),
+        (3, 2), (3, 2), (3, 2), (3, 2), (3, X - 1), (3, X - 1), (1,), (1,), (1,), (1,), (2,), (2,),
+        (2, 2), (2, 2), (2,), (2,), (1,), (HALF,), (1,), (1,), (1,), (1,),
     ):
-        scratch += [DMA(shape), DMA(shape)]
+        scratch.append(DMA(shape))
     return pl.pallas_call(
         functools.partial(layer_kernel, Z, X, paired),
         out_shape=jax.ShapeDtypeStruct((share, W), bf),

time: 152 us -> 135 us (0.89)
  Pallas kernels: 149 us -> 133 us
    pallas_call x1, Pallas kernels: 149 us -> 133 us  [fused_layer(): pl.pallas_call(functools.partial(layer_kernel, Z, X, paired), out_shape=j...]
where the time goes in v3:
time: 135 us
  Pallas kernels  133 us (99%)
  local copies, waits for them, and re-layouts  1.67 us (1%)
    pallas_call x1, Pallas kernels, fused_layer(): pl.pallas_call(functools.partial(layer_kernel, Z, X, paired), out_shape=j...  133 us

profile of v3, /device:TPU:33, one launch (start us, length us, event | category | flops | bytes accessed | tf_op | source)
XLA Modules:
  0.0 135.1 jit_solution(7805291451239954193)
XLA Ops:
  0.0 0.8 multiply_sine_fusion
  0.8 132.6 %layer.1 = bf16[64,2048]{1,0:T(8,128)(2,1)} custom-call(bf16[256,512]{1,0:T(8,128)(2,1)} %kvl.1, bf16[32,256]{1,0:T(8,128)(2,1)} %bitcast.6, bf16[64,2048]{1,0:T(8,128)(2,1)} %up_own.1, bf16[64,2048]{1,0:T(8,128)(2,1)} %bitcast.5, bf16[256,2048]{1,0:T(8,128)(2,1)} %hid.1, bf16[256,768]{1,0:T(8,128)(2,1)} %ql.1, bf16[768,384]{1,0:T(8,128)(2,1)} %wq.1, ...), custom_call_target="tpu_custom_call" | custom-call | tf_op jit(solution)/shard_map/layer/pallas_call | solution.py:708
  133.4 1.7 %copy.14 = bf16[64,2048]{1,0:T(8,128)(2,1)} copy(bf16[64,2048]{1,0:T(8,128)(2,1)} %layer.1) | data formatting | bytes 524288
  (2 shorter events, 0.0 us)

commit v4 on v3

--- a/solution.py
+++ b/solution.py
@@ -129,35 +129,37 @@
     xb[z, c, KB * share:, :] = packed_key.astype(bf)
     pl.semaphore_wait(barrier, len(peers))
 
-    def lz_copy(zz, hop, dev):
-        piece = xb.at[zz, c]
-        return rcopy(piece, piece, lz_s.at[0], lz_r.at[hop], dev)
+    cuts = (KB * share // 2, KB * share // 2 + grow)
+
+    def lz_copy(zz, hop, dev, n):
+        piece = xb.at[zz, c, pl.ds(n * cuts[0], cuts[n])]
+        return rcopy(piece, piece, lz_s.at[0], lz_r.at[n, hop], dev)
 
     def ld_copy(zz, t):
         return rcopy(xb.at[zz, c], xb.at[zz, c], ld_s.at[0], ld_r.at[t], sib)
 
-    def lz_wait(hop, count):
-        pieces = xb.at[pl.ds(0, count), 0]
-        rcopy(pieces, pieces, lz_s.at[0], lz_r.at[hop], sib).wait_recv()
+    def lz_wait(hop, count, n):
+        pieces = xb.at[pl.ds(0, count), 0, pl.ds(n * cuts[0], cuts[n])]
+        rcopy(pieces, pieces, lz_s.at[0], lz_r.at[n, hop], sib).wait_recv()
 
     def ld_wait(t):
         rcopy(xb.at[0], xb.at[0], ld_s.at[0], ld_r.at[t], sib).wait_recv()
 
     def lz_step(i):
         i = jnp.int32(i)
-
-        @pl.when(i < HALF)
-        def _():
-            lz_wait(i, 2)
-
-        @pl.when(i < HALF - 1)
-        def _():
-            lz_copy(at(z - i), i + 1, zdev(z + 1)).start()
-            lz_copy(at(z + i), i + 1, zdev(z - 1)).start()
-
-        @pl.when(i == HALF - 1)
-        def _():
-            lz_copy(at(z - i * sgn), i + 1, zdev(z + sgn)).start()
+        for n in range(2):
+            pl.when(i < HALF)(lambda: lz_wait(i, 2, n))
+
+            @pl.when(i < HALF - 1)
+            def _():
+                lz_copy(at(z - i), i + 1, zdev(z + 1), n).start()
+                lz_copy(at(z + i), i + 1, zdev(z - 1), n).start()
+
+            @pl.when(i == HALF - 1)
+            def _():
+                lz_copy(at(z - i * sgn), i + 1, zdev(z + sgn), n).start()
+
+            pl.when(i == HALF)(lambda: lz_wait(i, 1, n))
 
         @pl.when(i < HALF)
         def _():
@@ -166,7 +168,6 @@
 
         @pl.when(i == HALF)
         def _():
-            lz_wait(i, 1)
             ld_copy(at(z + HALF), i).start()
 
     kv_half, q_half, o_half = WKV.shape[1] // 2, qx.shape[2], WO.shape[1] // 2
@@ -222,19 +223,21 @@
                 xd_copy(what, n).wait_recv()
 
     weights = (U, D)
-    ZW = 3 if paired else 4
+    ZW = (2, 3) if paired else (4, 4)
     part = shard // 4
-    NP = ZW * HALF
-
-    def place(zz, turn):
-        return pl.ds(pl.multiple_of(shard_at(zz, c) + part * turn, part), part)
+    NP = tuple(ways * HALF for ways in ZW)
+
+    def place(zz, turn, count=1):
+        return pl.ds(pl.multiple_of(shard_at(zz, c) + part * turn, part), part * count)
 
     def z_piece(arr, zz, k):
-        s = lax.rem(k, ZW)
-        return weights[arr].at[place(zz, jnp.where(s == 2, 2 + par, s) if paired else s)]
+        s = lax.rem(k, ZW[arr])
+        if paired:
+            s = 2 * par + s if arr == 0 else jnp.where(s == 2, 2 + par, s)
+        return weights[arr].at[place(zz, s)]
 
     def y_piece(arr, zz, turn):
-        return weights[arr].at[place(zz, 2 + turn)]
+        return weights[arr].at[place(zz, 2 * turn, 2) if arr == 0 else place(zz, 2 + turn)]
 
     def wz_copy(arr, zz, k, dev):
         piece = z_piece(arr, zz, k)
@@ -254,11 +257,12 @@
         rcopy(w_rows(count * part), w_rows(count * part), w_s.at[0], wz_r.at[arr, k], sib).wait_recv()
 
     def wy_wait(arr, hop, count):
+        count = count * (4 - ZW[arr])
         rcopy(w_rows(count * part), w_rows(count * part), w_s.at[0], wy_r.at[arr, hop], sib).wait_recv()
 
     def w_first(arr):
         to_sib(arr, weights[arr].at[pl.ds(shard_at(z, c), shard)], HALF).start()
-        for k in range(ZW):
+        for k in range(ZW[arr]):
             wz_copy(arr, z, jnp.int32(k), zdev(z + 1)).start()
             wz_copy(arr, z, jnp.int32(k), zdev(z - 1)).start()
 
@@ -278,8 +282,8 @@
 
     def w_serve(arr, k):
         k = jnp.int32(k)
-        hop = k // ZW + 1
-        last_way = lax.rem(k, ZW) == 2
+        hop = k // ZW[arr] + 1
+        last_way = lax.rem(k, ZW[arr]) == ZW[arr] - 1
 
         @pl.when(hop < HALF)
         def _():
@@ -287,12 +291,12 @@
 
         @pl.when(hop < HALF - 1)
         def _():
-            wz_copy(arr, at(z - hop), k + ZW, zdev(z + 1)).start()
-            wz_copy(arr, at(z + hop), k + ZW, zdev(z - 1)).start()
+            wz_copy(arr, at(z - hop), k + ZW[arr], zdev(z + 1)).start()
+            wz_copy(arr, at(z + hop), k + ZW[arr], zdev(z - 1)).start()
 
         @pl.when(hop == HALF - 1)
         def _():
-            wz_copy(arr, at(z - hop * sgn), k + ZW, zdev(z + sgn)).start()
+            wz_copy(arr, at(z - hop * sgn), k + ZW[arr], zdev(z + sgn)).start()
 
         @pl.when(hop < HALF)
         def _():
@@ -312,34 +316,41 @@
                 pl.when(last_way)(lambda: wy_copy(arr, at(z + HALF), hop, par).start())
 
         if arr == 0:
-            pl.when(k == NP - ZW - 1)(lambda: w_first(1))
-        if paired:
-            pl.when((lax.rem(k, ZW) == 0) & (hop > 2))(lambda: y_serve(arr, hop - 2))
+            pl.when(k == ZW[0] * (AHEAD - 1))(lambda: w_first(1))
 
     served = [0]
     y_done = [0, 0]
-
-    def count_y(arr, count):
-        y_done[arr] = max(y_done[arr], (count - 1) // ZW - 1)
 
     def need_y(arr, hop):
         while paired and y_done[arr] < hop:
             y_done[arr] += 1
             y_serve(arr, y_done[arr])
 
+    AHEAD = min(4, HALF)
+    order = []
+    for hop in range(HALF):
+        order += [(0, ZW[0] * hop + n) for n in range(ZW[0])]
+        if hop >= AHEAD:
+            order += [(1, ZW[1] * (hop - AHEAD) + n) for n in range(ZW[1])]
+    order += [(1, k) for k in range(ZW[1] * (HALF - AHEAD), NP[1])]
+
     def serve(count):
         for _ in range(count):
-            if served[0] == 2 * NP:
+            if served[0] == len(order):
                 return
-            arr, k = served[0] // NP, served[0] % NP
+            arr, k = order[served[0]]
             w_serve(arr, k)
-            count_y(arr, k + 1)
             served[0] += 1
-            if arr == 1 and k in (0, 2):
-                need_y(0, HALF - 1 if k == 0 else HALF)
-
-    lz_copy(z, 1, zdev(z + 1)).start()
-    lz_copy(z, 1, zdev(z - 1)).start()
+            if arr == 1 and k % ZW[1] == 0:
+                need_y(1, k // ZW[1] - 1)
+
+    def serve_until(arr, hop):
+        while served[0] <= order.index((arr, ZW[arr] * min(hop, HALF) - 1)):
+            serve(1)
+
+    for n in range(2):
+        lz_copy(z, 1, zdev(z + 1), n).start()
+        lz_copy(z, 1, zdev(z - 1), n).start()
     ld_copy(z, HALF).start()
     for load in (loads[0], loads[1], loads[3]):
         load.wait()
@@ -363,18 +374,23 @@
     l_sc[...] = jnp.zeros_like(l_sc)
     o_sc[...] = jnp.zeros_like(o_sc)
 
-    lz_step(1)
+    begun = 0
+
+    def lz_next():
+        nonlocal begun
+        if begun < min(5, HALF - 1):
+            begun += 1
+            lz_step(begun)
+            serve(1)
+
     loads[4].wait()
+    lz_next()
     x_relay(0)
-    serve(1)
-    if HALF > 2:
-        lz_step(2)
-        serve(1)
+    lz_next()
     x_relay(1)
+    lz_next()
     x_share(0)
-    if HALF > 3:
-        lz_step(3)
-        serve(1)
+    lz_next()
     x_share(1)
     loads[2].wait()
     x_first(2)
@@ -387,8 +403,7 @@
             key_rows.append(by_row[h * step:h * step + PLAIN])
             wvt[(jj * HP + h) * VALUE:(jj * HP + h + 1) * VALUE, :] = by_row[h * step + PLAIN:(h + 1) * step].astype(bf)
     wk[...] = jnp.transpose(jnp.concatenate(key_rows, axis=0)).astype(bf)
-    if HALF > 3:
-        serve(2)
+    lz_next()
     x_end(1)
     for jj in range(X // 2):
         for h in range(HP):
@@ -398,7 +413,6 @@
                 lanes = slice((2 * hh + cc) * T, (2 * hh + cc + 1) * T)
                 q2t[p, hh * PLAIN:(hh + 1) * PLAIN, lanes] = qx[c * (X // 2) + jj, cc, h * wide:h * wide + PLAIN, :]
                 q2t[p, LANES:LANES + ROTARY, lanes] = qx[c * (X // 2) + jj, cc, h * wide + PLAIN:(h + 1) * wide, :]
-    begun = 3 if HALF > 3 else HALF - 1 if HALF > 2 else 1
 
     def attend(za, zb):
         lhs = jnp.concatenate(
@@ -419,9 +433,14 @@
         rope = jnp.concatenate(rope, axis=0).astype(bf)
         kk = jnp.dot(lhs, wk[...], preferred_element_type=f32).astype(bf)
         vt = nt_dot(wvt[...], lhs).astype(bf)
-        for p in range(HC // 2):
+        def scores(p):
             k2 = jnp.concatenate([kk[:, p * LANES:(p + 1) * LANES], rope], axis=1)
             s_buf[p] = jnp.dot(k2, q2t[p], preferred_element_type=f32)
+
+        scores(0)
+        for p in range(HC // 2):
+            if p + 1 < HC // 2:
+                scores(p + 1)
             old = m_sc[p:p + 1, :]
             new = jnp.maximum(old, jnp.max(s_buf[p], axis=0, keepdims=True))
             factor = jnp.exp2(old - new)
@@ -438,14 +457,17 @@
 
     base = served[0]
     rounds = HALF // 2
+    turn = ZW[0] * min(AHEAD + 1, HALF)
 
     def phase(u, carry):
         for s in range(2):
             t = 2 * u + 1 + s
             pl.when(t + begun <= HALF)(lambda: lz_step(t + begun))
-            for n in range(2):
-                k = base + 2 * (t - 1) + n
-                pl.when(k < NP)(lambda: w_serve(0, k))
+            k = base + t - 1
+            pl.when(k < turn)(lambda: w_serve(0, k))
+            pl.when(k >= turn)(lambda: w_serve(1, jnp.maximum(k - turn, 0)))
+            if paired and s == 1:
+                y_serve(0, u + 1)
             if s == 0:
                 pl.when(u == min(1, rounds - 1))(lambda: x_relay(2))
             else:
@@ -456,8 +478,8 @@
         return carry
 
     lax.fori_loop(0, rounds, phase, 0)
-    served[0] = min(base + 2 * HALF, NP)
-    count_y(0, served[0])
+    served[0] = base + HALF
+    y_done[0] = rounds
 
     heads = []
     for h in range(HC):
@@ -497,7 +519,7 @@
     for copy in far + near:
         copy.start()
     orx[here] = obuf[x, c]
-    serve(3)
+    serve(4)
     for i, d in enumerate((1, -1)):
         far[i].wait_recv()
         rcopy(relay.at[i], orx.at[2 * xat(-d) + c], mo_s.at[0], mo_r.at[0], owner(d, i)).start()
@@ -516,7 +538,8 @@
         coefs += [part_of * norm for part_of in parts]
     wts[...] = jnp.transpose(jnp.concatenate(coefs, axis=0))
     x_end(2)
-    serve(3)
+    serve(4)
+    need_y(0, HALF - 3)
     seven(orx, mo_s, mo_r).wait_recv()
     columns = wts[rowsof(x), :]
     for core in range(2):
@@ -549,7 +572,8 @@
     spread = [[spread_copy(n, i, d) for i, d in enumerate((1, -1))] for n in range(2)]
     for copy in spread[0] + spread[1]:
         copy.start()
-    serve(4)
+    need_y(0, HALF - 2)
+    serve(5)
     onward = []
     for i, d in enumerate((1, -1)):
         spread[0][i].wait_recv()
@@ -557,14 +581,15 @@
         onward.append(rcopy(piece, piece, ah_s.at[i], ah_r.at[i], xdev(d)))
         onward[-1].start()
     serve(4)
+    need_y(0, HALF - 1)
+    serve(1)
     for copy in spread[1] + onward:
         copy.wait_recv()
 
     def wd_wait(arr, hop, count):
         rcopy(w_rows(count), w_rows(count), w_s.at[1], wd_r.at[0 if arr == 0 else hop], sib).wait_recv()
 
-    while served[0] < NP:
-        serve(1)
+    serve_until(0, HALF)
     need_y(0, HALF)
     wd_wait(0, 0, Z * shard)
     CUTS = 4
@@ -576,7 +601,7 @@
             act[:, cols] = (high * high).astype(bf)
             return carry
         lax.fori_loop(stage * per, (stage + 1) * per, up, 0)
-        serve(1)
+        serve(2)
 
     def fa_copy(t, i, d):
         return rcopy(osend.at[t, xat(2), i], opart.at[t, i], fa_s.at[0], fa_r.at[t], xdev(d))
@@ -584,6 +609,7 @@
     def fo_copy(t, i, d):
         return rcopy(osend.at[t, xat(d)], orecv.at[t, i], fo_s.at[0], fo_r.at[0], xdev(d))
 
+    LAG = 3
     direct = rcopy(osend.at[HALF - 1, xat(2)], ofar, fz_s.at[0], fz_r.at[0], xdev(2))
 
     def pair_of(t):
@@ -596,8 +622,7 @@
             fo_copy(t, i, d).start()
 
     for t in range(1, HALF + 1):
-        while served[0] < min(NP + ZW * (t + 1) + 1, 2 * NP):
-            serve(1)
+        serve_until(1, t + 1)
         need_y(1, t)
         wd_wait(1, t, 2 * shard)
         rhs = jnp.concatenate(
@@ -614,8 +639,10 @@
             direct.start()
             for i, d in enumerate((1, -1)):
                 fo_copy(t - 1, i, d).start()
-        if t > 1:
-            pass_on(t - 2)
+        if t > LAG:
+            pass_on(t - 1 - LAG)
+    for t in range(max(HALF - LAG, 0), HALF - 1):
+        pass_on(t)
     rcopy(orecv, orecv, fo_s.at[0], fo_r.at[0], sib).wait_recv()
     direct.wait_recv()
     for t in range(1, HALF + 1):
@@ -645,7 +672,7 @@
             else:
                 xd_copy(what, n).wait_send()
     sent = xb.at[pl.ds(0, Z - 1), 0]
-    rcopy(sent, sent, lz_s.at[0], lz_r.at[0], sib).wait_send()
+    rcopy(sent, sent, lz_s.at[0], lz_r.at[0, 0], sib).wait_send()
     sent = xb.at[pl.ds(0, HALF)]
     rcopy(sent, sent, ld_s.at[0], ld_r.at[0], sib).wait_send()
     sent = w_rows(2 * (Z - 1) * 4 * part)
@@ -699,8 +726,8 @@
         DMA((5,)),
     ]
     for shape in (
-        (1,), (HALF + 1,), (1,), (HALF + 1,),
-        (2,), (2, 4 * HALF if not paired else 3 * HALF), (2, HALF + 1), (HALF + 1,),
+        (1,), (2, HALF + 1), (1,), (HALF + 1,),
+        (2,), (2, 4 * HALF), (2, HALF + 1), (HALF + 1,),
         (3, 2), (3, 2), (3, 2), (3, 2), (3, X - 1), (3, X - 1), (1,), (1,), (1,), (1,), (2,), (2,),
         (2, 2), (2, 2), (2,), (2,), (1,), (HALF,), (1,), (1,), (1,), (1,),
     ):

time: 135 us -> 126 us (0.933)
  Pallas kernels: 133 us -> 123 us
    pallas_call x1, Pallas kernels: 133 us -> 123 us  [fused_layer(): pl.pallas_call(functools.partial(layer_kernel, Z, X, paired), out_shape=j...]
where the time goes in v4:
time: 126 us
  Pallas kernels  123 us (98%)
  local copies, waits for them, and re-layouts  1.67 us (1%)
    pallas_call x1, Pallas kernels, fused_layer(): pl.pallas_call(functools.partial(layer_kernel, Z, X, paired), out_shape=j...  123 us

profile of v4, /device:TPU:33, one launch (start us, length us, event | category | flops | bytes accessed | tf_op | source)
XLA Modules:
  0.0 125.8 jit_solution(16930753355731023558)
XLA Ops:
  0.0 0.8 multiply_sine_fusion
  0.8 123.4 %layer.1 = bf16[64,2048]{1,0:T(8,128)(2,1)} custom-call(bf16[256,512]{1,0:T(8,128)(2,1)} %kvl.1, bf16[32,256]{1,0:T(8,128)(2,1)} %bitcast.6, bf16[64,2048]{1,0:T(8,128)(2,1)} %up_own.1, bf16[64,2048]{1,0:T(8,128)(2,1)} %bitcast.5, bf16[256,2048]{1,0:T(8,128)(2,1)} %hid.1, bf16[256,768]{1,0:T(8,128)(2,1)} %ql.1, bf16[768,384]{1,0:T(8,128)(2,1)} %wq.1, ...), custom_call_target="tpu_custom_call" | custom-call | tf_op jit(solution)/shard_map/layer/pallas_call | solution.py:735
  124.2 1.7 %copy.14 = bf16[64,2048]{1,0:T(8,128)(2,1)} copy(bf16[64,2048]{1,0:T(8,128)(2,1)} %layer.1) | data formatting | bytes 524288
  (2 shorter events, 0.0 us)

commit v5 on v4

--- a/solution.py
+++ b/solution.py
@@ -280,6 +280,13 @@
             wy_wait(arr, hop, 1)
             to_sib(arr, y_piece(arr, at(z + HALF), 1 - par), hop).start()
 
+    AHEAD = min(4, HALF)
+    LATER = max(HALF - AHEAD - 1, 0)
+
+    def y_send(arr, hop):
+        for side in range(2):
+            wy_copy(arr, zside(side, hop), hop, par).start()
+
     def w_serve(arr, k):
         k = jnp.int32(k)
         hop = k // ZW[arr] + 1
@@ -303,10 +310,9 @@
             for side in range(2):
                 to_sib(arr, z_piece(arr, zside(side, hop), k), hop).start()
             if paired:
-                @pl.when(last_way)
+                @pl.when(last_way & (hop > LATER) if arr == 1 else last_way)
                 def _():
-                    for side in range(2):
-                        wy_copy(arr, zside(side, hop), hop, par).start()
+                    y_send(arr, hop)
 
         @pl.when(hop == HALF)
         def _():
@@ -326,7 +332,6 @@
             y_done[arr] += 1
             y_serve(arr, y_done[arr])
 
-    AHEAD = min(4, HALF)
     order = []
     for hop in range(HALF):
         order += [(0, ZW[0] * hop + n) for n in range(ZW[0])]
@@ -341,8 +346,11 @@
             arr, k = order[served[0]]
             w_serve(arr, k)
             served[0] += 1
+            if (arr, k) == (0, NP[0] - 1) and paired:
+                for hop in range(1, LATER + 1):
+                    y_send(1, jnp.int32(hop))
             if arr == 1 and k % ZW[1] == 0:
-                need_y(1, k // ZW[1] - 1)
+                need_y(1, k // ZW[1] - 3)
 
     def serve_until(arr, hop):
         while served[0] <= order.index((arr, ZW[arr] * min(hop, HALF) - 1)):
@@ -601,7 +609,8 @@
             act[:, cols] = (high * high).astype(bf)
             return carry
         lax.fori_loop(stage * per, (stage + 1) * per, up, 0)
-        serve(2)
+        if stage < CUTS - 1:
+            serve(1)
 
     def fa_copy(t, i, d):
         return rcopy(osend.at[t, xat(2), i], opart.at[t, i], fa_s.at[0], fa_r.at[t], xdev(d))
@@ -622,6 +631,8 @@
             fo_copy(t, i, d).start()
 
     for t in range(1, HALF + 1):
+        if 1 < t <= HALF // 2:
+            serve(1)
         serve_until(1, t + 1)
         need_y(1, t)
         wd_wait(1, t, 2 * shard)

time: 126 us -> 124 us (0.984)
    pallas_call x1, Pallas kernels: 123 us -> 122 us  [fused_layer(): pl.pallas_call(functools.partial(layer_kernel, Z, X, paired), out_shape=j...]
where the time goes in v5:
time: 124 us
  Pallas kernels  122 us (98%)
  local copies, waits for them, and re-layouts  1.67 us (1%)
    pallas_call x1, Pallas kernels, fused_layer(): pl.pallas_call(functools.partial(layer_kernel, Z, X, paired), out_shape=j...  122 us

profile of v5, /device:TPU:33, one launch (start us, length us, event | category | flops | bytes accessed | tf_op | source)
XLA Modules:
  0.0 124.3 jit_solution(18135622034482324723)
XLA Ops:
  0.0 0.8 multiply_sine_fusion
  0.8 121.9 %layer.1 = bf16[64,2048]{1,0:T(8,128)(2,1)} custom-call(bf16[256,512]{1,0:T(8,128)(2,1)} %kvl.1, bf16[32,256]{1,0:T(8,128)(2,1)} %bitcast.6, bf16[64,2048]{1,0:T(8,128)(2,1)} %up_own.1, bf16[64,2048]{1,0:T(8,128)(2,1)} %bitcast.5, bf16[256,2048]{1,0:T(8,128)(2,1)} %hid.1, bf16[256,768]{1,0:T(8,128)(2,1)} %ql.1, bf16[768,384]{1,0:T(8,128)(2,1)} %wq.1, ...), custom_call_target="tpu_custom_call" | custom-call | tf_op jit(solution)/shard_map/layer/pallas_call | solution.py:746
  122.6 1.7 %copy.14 = bf16[64,2048]{1,0:T(8,128)(2,1)} copy(bf16[64,2048]{1,0:T(8,128)(2,1)} %layer.1) | data formatting | bytes 524288
  (2 shorter events, 0.0 us)
